TPU v7x, 512 devices: a whole 4x8x8 slice. The times are simulated.
512 devices in a mesh: ep: 32 (over z, x), tp: 16 (over y, core).
Axes of the slice: x: 4, y: 8, z: 8, core: 2. Of those that a mesh axis runs over, the one named last changes fastest.
Arguments:
- mixer_input: bfloat16 [4096, 2048], P('ep'), may hold values from -6 to 6
- mixer_gain: float32 [2048], replicated, may hold values from 0.1 to 1.9
- query_weight: bfloat16 [2048, 2048], P(None, 'tp'), may hold values from -0.125 to 0.125
- key_weight: bfloat16 [2048, 2048], P(None, 'tp'), may hold values from -0.125 to 0.125
- value_weight: bfloat16 [2048, 2048], P(None, 'tp'), may hold values from -0.125 to 0.125
- score_offset: float32 [16], P('tp'), may hold values from -8.6 to -4
- out_weight: bfloat16 [2048, 2048], P(None, 'tp'), may hold values from -1.3203125 to 1.3203125
- expert_input: bfloat16 [4096, 2048], P('ep'), may hold values from -6 to 6
- expert_gain: float32 [2048], replicated, may hold values from 0.1 to 1.9
- route_ids: int32 [4096, 2], P('ep'), may hold values from 0 to 31, as said below
- route_weights: float32 [4096, 2], P('ep'), may hold values from 0.1 to 1
- gate_weight: bfloat16 [32, 2048, 2048], P('ep', None, 'tp'), may hold values from -0.125 to 0.125
- up_weight: bfloat16 [32, 2048, 2048], P('ep', None, 'tp'), may hold values from -0.125 to 0.125
- down_weight: bfloat16 [32, 2048, 2048], P('ep', 'tp'), may hold values from -0.1875 to 0.1875
Outputs:
- mixer_output: bfloat16 [4096, 2048], P('ep', 'tp')
- expert_output: bfloat16 [4096, 2048], P('ep', 'tp')
Inputs may be any that keep to these rules, and one draw needn't show every extreme that they name: `route_ids`: each row names two different experts of one group; group g holds experts g * 8 to g * 8 + 7. Among the rows of one ep index no expert is named more than 16 times, and in every draw the experts of some group are each named exactly 16 times by the rows of every ep index.
All inputs are finite; a program needn't handle non-finite values.
Results may differ from a plain program's by a relative error of at most 0.019.
Values may be sent and summed in bfloat16 or wider, within the bound.
A program may use at most 64 MiB of HBM per device.

v0:
```python
import jax
import jax.numpy as jnp
from jax import lax
from jax.sharding import PartitionSpec as P

HD = 128
SUB = 64
GROUPS = 4


epsilon = 1e-06


def in_one_piece(arrays, axis, dim, along):
    both = jnp.concatenate(arrays, axis=along)
    filled, at, finished = (lax.all_gather(both, axis, axis=dim, tiled=True), 0, [])
    for a in arrays:
        finished.append(lax.slice_in_dim(filled, at, at + a.shape[along], axis=along))
        at += a.shape[along]
    return tuple(finished)


def cut_along(x, dim, devices):
    before, after = (x.shape[:dim], x.shape[dim + 1 :])
    return jnp.moveaxis(x.reshape(*before, devices, -1, *after), dim, 0)


def summed_on_arrival(x, axis, dim):
    devices = lax.axis_size(axis)
    pieces = lax.all_to_all(cut_along(x, dim, devices), axis, 0, 0, tiled=True)
    return jnp.sum(pieces.astype(jnp.float32), axis=0)


def rms_rows(rows_in, gain):
    values_f = rows_in.astype(jnp.float32)
    scaled = values_f * lax.rsqrt(jnp.mean(values_f * values_f, axis=-1, keepdims=True) + epsilon)
    return (scaled * gain).astype(jnp.bfloat16)


def token_mixer(
    mixer_input, mixer_gain, query_weight, key_weight, value_weight, score_offset, out_weight
):
    rows_here = mixer_input.shape[0]
    normed = rms_rows(mixer_input, mixer_gain)
    queries = jnp.dot(normed, query_weight, preferred_element_type=jnp.float32).astype(jnp.bfloat16)
    key_rows = jnp.dot(normed, key_weight, preferred_element_type=jnp.float32).astype(jnp.bfloat16)
    value_rows = jnp.dot(normed, value_weight, preferred_element_type=jnp.float32).astype(
        jnp.bfloat16
    )
    heads_here = queries.shape[1] // HD
    blocks = lax.axis_size("ep")
    my_block = lax.axis_index("ep")
    suffix_ones = jnp.tril(jnp.ones((SUB, SUB), jnp.float32))
    query_sets = (
        (queries, my_block * rows_here + jnp.arange(rows_here, dtype=jnp.int32), my_block),
    )

    def attend_set(query_flat, query_pos, key_heads, value_heads, shards):
        query_count = query_flat.shape[0]
        query_heads = query_flat.reshape(query_count, heads_here, HD)
        scores = jnp.einsum(
            "qhd,bkhd->bhqk", query_heads, key_heads, preferred_element_type=jnp.float32
        )
        scores = scores * HD ** (-0.5) + score_offset[None, :, None, None]
        key_pos = jnp.arange(shards * rows_here, dtype=jnp.int32).reshape(shards, 1, 1, rows_here)
        causal = key_pos < query_pos.reshape(1, 1, query_count, 1)
        log_keep = jnp.where(causal, jax.nn.log_sigmoid(-scores), 0.0)
        within = jnp.einsum(
            "bhqns,sr->bhqnr",
            log_keep.reshape(shards, heads_here, query_count, rows_here // SUB, SUB),
            suffix_ones,
        )
        sub_total = within[..., 0]
        later_subs = lax.cumsum(sub_total, axis=3, reverse=True) - sub_total
        after_sum = (within + later_subs[..., None]).reshape(
            shards, heads_here, query_count, rows_here
        ) - log_keep
        weights = jnp.where(causal, jnp.exp(jax.nn.log_sigmoid(scores) + after_sum), 0.0).astype(
            jnp.bfloat16
        )
        block_part = jnp.einsum(
            "bhqk,bkhd->bqhd", weights, value_heads, preferred_element_type=jnp.float32
        )
        keep_part = jnp.sum(sub_total, axis=3).transpose(0, 2, 1)
        return (block_part, keep_part)

    def bind_attend(query_flat, query_pos, key_heads, value_heads, shards):

        def attend(state_in):
            return attend_set(query_flat, query_pos, key_heads, value_heads, shards)

        return attend

    def untouched(state_in):
        return state_in

    initial = tuple(
        (
            (
                jnp.zeros((blocks, entry[0].shape[0], heads_here, HD), jnp.float32),
                jnp.zeros((blocks, entry[0].shape[0], heads_here), jnp.float32),
            )
            for entry in query_sets
        )
    )
    key_part, value_part = in_one_piece((key_rows, value_rows), "ep", 0, 1)
    shards = key_part.shape[0] // rows_here
    first_block = jnp.int32(0) // rows_here
    key_heads = key_part.reshape(shards, rows_here, heads_here, HD)
    value_heads = value_part.reshape(shards, rows_here, heads_here, HD)
    updated = []
    for (query_flat, query_pos, limit), state_in in zip(query_sets, initial):
        attend = bind_attend(query_flat, query_pos, key_heads, value_heads, shards)
        updated.append(lax.cond(first_block <= limit, attend, untouched, state_in))
    folded = tuple(updated)
    finished = []
    for block_out, block_keep in folded:
        later_keep = lax.cumsum(block_keep, axis=0, reverse=True) - block_keep
        summed = jnp.sum(jnp.exp(later_keep)[..., None] * block_out, axis=0)
        finished.append(summed.astype(jnp.bfloat16).reshape(block_out.shape[1], heads_here * HD))
    attended = finished[0]
    mixed_out = jnp.dot(
        lax.all_gather(attended, "tp", axis=1, tiled=True),
        out_weight,
        preferred_element_type=jnp.float32,
    )
    return mixed_out.astype(jnp.bfloat16)


def finish_expert(gate_sum, up_sum, sources, slot_count, down_weight):
    hidden = (jax.nn.silu(gate_sum) * up_sum).astype(jnp.bfloat16)
    partial_out = jnp.dot(hidden, down_weight[0], preferred_element_type=jnp.float32)
    partial_out = partial_out.reshape(sources, slot_count, partial_out.shape[1])
    summed = summed_on_arrival(partial_out.astype(jnp.bfloat16), "tp", 2).astype(jnp.bfloat16)
    return lax.all_to_all(summed, "ep", split_axis=0, concat_axis=0, tiled=True)


def routed_experts(
    expert_input, expert_gain, route_ids, route_weights, gate_weight, up_weight, down_weight
):
    rows_here = expert_input.shape[0]
    model_width = expert_input.shape[1]
    normed = rms_rows(expert_input, expert_gain)
    experts = lax.axis_size("ep")
    capacity = rows_here // (experts // GROUPS)
    flat_ids = route_ids.reshape(-1)
    onehot = (flat_ids[:, None] == jnp.arange(experts, dtype=jnp.int32)[None, :]).astype(jnp.int32)
    slot_index = jnp.sum((jnp.cumsum(onehot, axis=0) - 1) * onehot, axis=1)
    target = flat_ids * capacity + slot_index
    assign_row = jnp.arange(flat_ids.shape[0], dtype=jnp.int32) // 2
    source_row = jnp.full((experts * capacity,), rows_here, jnp.int32).at[target].set(assign_row)
    padded = jnp.concatenate([normed, jnp.zeros((1, model_width), jnp.bfloat16)], axis=0)
    outgoing = padded[source_row].reshape(experts, capacity, model_width)
    arrived = lax.all_to_all(outgoing, "ep", split_axis=0, concat_axis=0, tiled=True)
    flat_rows = arrived.reshape(arrived.shape[0] * arrived.shape[1], model_width)
    gate_sum = jnp.dot(flat_rows, gate_weight[0], preferred_element_type=jnp.float32)
    up_sum = jnp.dot(flat_rows, up_weight[0], preferred_element_type=jnp.float32)
    returned = finish_expert(gate_sum, up_sum, arrived.shape[0], arrived.shape[1], down_weight)
    out_cols = returned.shape[2]
    picked = returned.reshape(experts * capacity, out_cols)[target].astype(jnp.float32)
    picked = picked.reshape(rows_here, 2, out_cols)
    combined = jnp.sum(route_weights[:, :, None] * picked, axis=1)
    return combined.astype(jnp.bfloat16)


def on_device(
    mixer_input,
    mixer_gain,
    query_weight,
    key_weight,
    value_weight,
    score_offset,
    out_weight,
    expert_input,
    expert_gain,
    route_ids,
    route_weights,
    gate_weight,
    up_weight,
    down_weight,
):
    mixer_output = token_mixer(
        mixer_input, mixer_gain, query_weight, key_weight, value_weight, score_offset, out_weight
    )
    expert_output = routed_experts(
        expert_input, expert_gain, route_ids, route_weights, gate_weight, up_weight, down_weight
    )
    return (mixer_output, expert_output)


def solution(mesh):
    in_specs = (
        P("ep", None),
        P(),
        P(None, "tp"),
        P(None, "tp"),
        P(None, "tp"),
        P("tp"),
        P(None, "tp"),
        P("ep", None),
        P(),
        P("ep", None),
        P("ep", None),
        P("ep", None, "tp"),
        P("ep", None, "tp"),
        P("ep", "tp", None),
    )
    out_specs = (P("ep", "tp"), P("ep", "tp"))
    return jax.shard_map(
        on_device, mesh=mesh, in_specs=in_specs, out_specs=out_specs, check_vma=False
    )
```

profile of v0, /device:TPU:1, one launch (start us, length us, event | category | flops | bytes accessed | tf_op | source)
XLA Modules:
  0.0 179.3 jit_solution(7195809973663508250)
XLA Ops:
  7.2 0.0 copy-start
  7.2 0.7 broadcast_multiply_fusion
  7.9 0.8 copy.37
  8.7 0.1 eq.29
  8.9 0.1 eq.25
  9.0 1.2 fusion.27
  10.2 0.1 copy.36
  10.3 0.1 mul.107
  10.5 0.6 reduce-window.6
  11.1 0.2 slice_reduce_fusion.1
  11.3 0.1 fusion.36
  11.4 1.4 scatter_custom_fusion
  12.9 1.2 fusion.29
  14.2 3.3 %gather_fusion = bf16[512,2048]{1,0:T(8,128)(2,1)} fusion(bf16[129,2048]{1,0:T(8,128)(2,1)S(1)} %concatenate.7, s32[1024]{0:T(1024)S(1)} %pad_clamp_fusion.1), kind=kCustom, calls=%fused_computation | custom fusion | bytes 4196352 | tf_op jit(solution)/shard_map/gather | solution.py:153
  17.5 0.0 copy-start.1
  17.5 0.0 copy-start.5
  17.5 13.8 %all-to-all-start = ((bf16[32,16,2048]{2,1,0:T(8,128)(2,1)}), bf16[32,16,2048]{2,1,0:T(8,128)(2,1)S(1)}, u32[]{:S(2)}, u32[]{:S(2)}) async-start(bf16[32,16,2048]{2,1,0:T(8,128)(2,1)} %bitcast.24), calls=%async_computation | async-start | bytes 4194304 | tf_op jit(solution)/shard_map/all_to_all | solution.py:154
  31.4 0.0 all-gather.2.cloned.1.call-start
  31.4 0.0 copy-done.1
  31.4 0.2 fusion.24
  31.6 0.0 copy-done.5
  31.6 1.4 convolution_convert_fusion.3
  33.1 1.4 convolution_convert_fusion.4
  34.5 0.6 pad_maximum_fusion
  35.2 0.0 all-gather.2.cloned.1.call-update
  35.2 47.1 %all-to-all-done = bf16[32,16,2048]{2,1,0:T(8,128)(2,1)S(1)} async-done(((bf16[32,16,2048]{2,1,0:T(8,128)(2,1)}), bf16[32,16,2048]{2,1,0:T(8,128)(2,1)S(1)}, u32[]{:S(2)}, u32[]{:S(2)}) %all-to-all-start) | async-done | bytes 2097184 | tf_op jit(solution)/shard_map/all_to_all | solution.py:154
  82.2 0.0 copy-start.4
  82.2 1.8 %fusion.32 = f32[512,128]{1,0:T(8,128)S(1)} fusion(bf16[512,2048]{1,0:T(8,128)(2,1)S(1)} %bitcast.113, bf16[1,2048,128]{2,1,0:T(8,128)(2,1)} %param.27), kind=kOutput, calls=%fused_computation.63 | convolution fusion | flops 268435456 | bytes 2883584 | tf_op jit(solution)/shard_map/dot_general | solution.py:156
  84.1 0.0 copy-done.4
  84.1 0.7 fusion.22
  84.8 0.0 copy-done
  84.8 0.7 fusion.21
  85.5 1.9 %copy.47 = bf16[32,2,16,8,128]{4,3,1,0,2:T(8,128)(2,1)} copy(bf16[32,2,16,8,128]{4,3,2,1,0:T(8,128)(2,1)S(1)} %fusion.21) | data formatting | bytes 4194304 | tf_op jit(solution)/shard_map/reshape | solution.py:25
  87.4 0.0 copy-start.3
  87.4 9.8 %all-to-all-start.1 = ((bf16[16,32,16,128]{3,2,1,0:T(8,128)(2,1)}), bf16[16,32,16,128]{3,2,1,0:T(8,128)(2,1)S(1)}, u32[]{:S(2)}, u32[]{:S(2)}) async-start(bf16[16,32,16,128]{3,2,1,0:T(8,128)(2,1)} %bitcast.112), calls=%async_computation.1 | async-start | bytes 4194304 | tf_op jit(solution)/shard_map/all_to_all | solution.py:30
  97.2 0.0 copy-done.3
  97.2 0.1 copy.35
  97.3 1.4 convolution_convert_fusion.2
  98.7 22.7 %all-gather.2.cloned.1.call-done = bf16[4096,256]{0,1:T(8,128)(2,1)} async-done(((bf16[128,256]{0,1:T(8,128)(2,1)}), bf16[4096,256]{0,1:T(8,128)(2,1)}) %all-gather.2.cloned.1.call-update) | async-done | bytes 2097168 | tf_op jit(solution)/shard_map/all_gather | solution.py:16
  121.4 15.2 %conditional.1 = (f32[32,128,1,128]{3,1,0,2:T(8,128)}, f32[32,128,1]{1,0,2:T(8,128)S(1)}) conditional(s32[]{:T(128)} %convert_element_type.59, () %tuple.16, (s32[]{:T(128)}, s32[128]{0:T(128)S(1)}, bf16[4096,256]{0,1:T(8,128)(2,1)}, bf16[128,128]{1,0:T(8,128)(2,1)S(1)}, f32[1]{0:T(128)}, /*index=5*/s32[64,64]{0,1:T(8,128)S(1)}, ...), branch_computations={%region_1.2_spmd, %region_2.5_spmd} | conditional | flops 353931392 | bytes 29624360 | solution.py:114
  121.4 4.1 %copy.32 = bf16[4096,256]{1,0:T(8,128)(2,1)} copy(bf16[4096,256]{0,1:T(8,128)(2,1)} %get-tuple-element.60) | data formatting | bytes 4194304 | tf_op jit(solution)/shard_map
  125.5 1.7 fusion.43
  127.2 2.6 %compare_select_fusion.3 = (bf16[32,1,128,128]{2,3,0,1:T(8,128)(2,1)S(1)}, f32[32,128,128]{2,1,0:T(8,128)S(1)}) fusion(f32[]{:T(128)} %bitcast.2, s32[128]{0:T(128)S(1)} %broadcast_add_fusion.1, s32[32,128]{1,0:T(8,128)S(1)} %multiply_add_fusion.1, bf16[32,128,128]{2,1,0:T(8,128)(2,1)S(1)} %bitcast.118, bf16[128,128]{1,0:T(8,128)(2,1)S(1)} %get-tuple-element.32), kind=kOutput, calls=%fused_computation.6 | convolution fusion | flops 139984896 | bytes 4243972 | tf_op jit(solution)/shard_map/cond/branch_1_fun/qhd,bkhd->bhqk/dot_general | solution.py:61
  129.8 0.4 fusion.10
  130.2 0.1 slice_reduce_fusion
  130.3 0.5 broadcast_add_fusion
  130.8 4.0 %fusion = bf16[32,1,128,128]{2,3,0,1:T(8,128)(2,1)S(1)} fusion(f32[32,128,2,64]{1,3,2,0:T(8,128)S(1)} %broadcast_add_fusion, f32[32,128,128]{2,1,0:T(8,128)S(1)} %get-tuple-element.68, f32[]{:T(128)} %bitcast.2, s32[128]{0:T(128)S(1)} %broadcast_add_fusion.1, s32[32,128]{1,0:T(8,128)S(1)} %multiply_add_fusion.1), kind=kLoop, calls=%fused_computation.7 | loop fusion | flops 12058624 | bytes 5259780 | tf_op jit(solution)/shard_map/cond/branch_1_fun/convert_element_type | solution.py:78
  134.8 1.9 %convolution_bitcast_fusion = f32[32,128,1,128]{3,1,0,2:T(8,128)} fusion(bf16[32,128,128]{2,1,0:T(8,128)(2,1)S(1)} %bitcast.115, bf16[32,1,128,128]{2,3,0,1:T(8,128)(2,1)S(1)} %fusion), kind=kOutput, calls=%fused_computation.21 | convolution fusion | flops 134217728 | bytes 4194304 | tf_op jit(solution)/shard_map/cond/branch_1_fun/bhqk,bkhd->bqhd/dot_general | solution.py:81
  136.6 0.1 fusion.23
  136.7 0.0 copy-start.2
  136.7 2.0 %multiply_reduce_fusion = bf16[128,128]{1,0:T(8,128)(2,1)S(1)} fusion(f32[32,128,1,128]{3,1,0,2:T(8,128)} %get-tuple-element.41, f32[32,128]{1,0:T(8,128)S(1)} %bitcast.124), kind=kLoop, calls=%fused_computation.41 | loop fusion | flops 1032192 | bytes 2146304 | tf_op jit(solution)/shard_map/reduce_sum | solution.py:119
  138.7 7.5 %all-to-all-done.1 = bf16[16,32,16,128]{3,2,1,0:T(8,128)(2,1)S(1)} async-done(((bf16[16,32,16,128]{3,2,1,0:T(8,128)(2,1)}), bf16[16,32,16,128]{3,2,1,0:T(8,128)(2,1)S(1)}, u32[]{:S(2)}, u32[]{:S(2)}) %all-to-all-start.1) | async-done | bytes 2097184 | tf_op jit(solution)/shard_map/all_to_all | solution.py:30
  146.2 0.9 reduce_sum.73
  147.1 5.2 %all-to-all-start.2 = ((bf16[32,16,128]{2,1,0:T(8,128)(2,1)}), bf16[32,16,128]{2,1,0:T(8,128)(2,1)S(1)}, u32[]{:S(2)}, u32[]{:S(2)}) async-start(bf16[32,16,128]{2,1,0:T(8,128)(2,1)} %reduce_sum.73), calls=%async_computation.2 | async-start | bytes 262144 | tf_op jit(solution)/shard_map/all_to_all | solution.py:135
  152.4 17.4 %all_gather.7 = bf16[128,2048]{1,0:T(8,128)(2,1)S(1)} all-gather(bf16[128,128]{1,0:T(8,128)(2,1)S(1)} %multiply_reduce_fusion), channel_id=1, replica_groups=mesh['ep'=32,'tp'=16] {'tp'}, dimensions={1}, use_global_device_ids=true | all-gather | bytes 557056 | tf_op jit(solution)/shard_map/all_gather | solution.py:123
  169.8 0.0 copy-done.2
  169.8 0.9 convolution_convert_fusion.1
  170.7 0.0 all-to-all-done.2
  170.7 0.9 gather_fusion.1
  171.6 0.9 fusion.34
  (17 shorter events, 0.2 us)
Async XLA Ops:
  7.2 77.6 %copy-start = (bf16[1,128,2048]{2,1,0:T(8,128)(2,1)S(1)}, bf16[1,128,2048]{2,1,0:T(8,128)(2,1)}, u32[]{:S(2)}) copy-start(bf16[1,128,2048]{2,1,0:T(8,128)(2,1)} %param.29) | copy-start | bytes 1572868
  17.5 13.9 %copy-start.1 = (bf16[128,2048]{1,0:T(8,128)(2,1)S(1)}, bf16[128,2048]{1,0:T(8,128)(2,1)}, u32[]{:S(2)}) copy-start(bf16[128,2048]{1,0:T(8,128)(2,1)} %param.16) | copy-start | bytes 1572868
  17.5 14.1 %copy-start.5 = (f32[2048]{0:T(1024)S(1)}, f32[2048]{0:T(1024)}, u32[]{:S(2)}) copy-start(f32[2048]{0:T(1024)} %param.17) | copy-start | bytes 24580
  17.5 64.7 %all-to-all-start = ((bf16[32,16,2048]{2,1,0:T(8,128)(2,1)}), bf16[32,16,2048]{2,1,0:T(8,128)(2,1)S(1)}, u32[]{:S(2)}, u32[]{:S(2)}) async-start(bf16[32,16,2048]{2,1,0:T(8,128)(2,1)} %bitcast.24), calls=%async_computation | async-start | bytes 4194304 | tf_op jit(solution)/shard_map/all_to_all | solution.py:154
  31.4 90.0 %all-gather.2.cloned.1.call-start = ((), (), s32[]{:S(2)}) async-start(), calls=%async_computation.3 | async-start | bytes 2162688 | tf_op jit(solution)/shard_map/all_gather | solution.py:16
  82.2 1.8 %copy-start.4 = (bf16[1,2048,128]{2,1,0:T(8,128)(2,1)S(1)}, bf16[1,2048,128]{2,1,0:T(8,128)(2,1)}, u32[]{:S(2)}) copy-start(bf16[1,2048,128]{2,1,0:T(8,128)(2,1)} %param.28) | copy-start | bytes 1572868
  87.4 9.8 %copy-start.3 = (f32[128,2]{0,1:T(2,128)S(1)}, f32[128,2]{0,1:T(2,128)}, u32[]{:S(2)}) copy-start(f32[128,2]{0,1:T(2,128)} %param.26) | copy-start | bytes 3076
  87.4 58.8 %all-to-all-start.1 = ((bf16[16,32,16,128]{3,2,1,0:T(8,128)(2,1)}), bf16[16,32,16,128]{3,2,1,0:T(8,128)(2,1)S(1)}, u32[]{:S(2)}, u32[]{:S(2)}) async-start(bf16[16,32,16,128]{3,2,1,0:T(8,128)(2,1)} %bitcast.112), calls=%async_computation.1 | async-start | bytes 4194304 | tf_op jit(solution)/shard_map/all_to_all | solution.py:30
  136.7 33.1 %copy-start.2 = (bf16[2048,128]{1,0:T(8,128)(2,1)S(1)}, bf16[2048,128]{1,0:T(8,128)(2,1)}, u32[]{:S(2)}) copy-start(bf16[2048,128]{1,0:T(8,128)(2,1)} %param.22) | copy-start | bytes 1572868
  147.1 23.6 %all-to-all-start.2 = ((bf16[32,16,128]{2,1,0:T(8,128)(2,1)}), bf16[32,16,128]{2,1,0:T(8,128)(2,1)S(1)}, u32[]{:S(2)}, u32[]{:S(2)}) async-start(bf16[32,16,128]{2,1,0:T(8,128)(2,1)} %reduce_sum.73), calls=%async_computation.2 | async-start | bytes 262144 | tf_op jit(solution)/shard_map/all_to_all | solution.py:135
Sparse Core Ops, SparseCore 0:
  35.3 86.0 all-gather.1
where the time goes:
time: 180 us; the launch traced here: 179 us
  waiting for transfers between devices  77.3 us (43%)
  starting transfers between devices  28.9 us (16%)
  blocking collectives  17.4 us (10%)
  local copies, waits for them, and re-layouts  15 us (8%)
  between operations  14.2 us (8%)
  other arithmetic  13.2 us (7%)
  matrix products  13.2 us (7%)
    all_to_all x1, waiting for transfers between devices, routed_experts(): lax.all_to_all(outgoing, 'ep', split_axis=0, concat_axis=0, tiled=True)  47.1 us
    all_gather x1, waiting for transfers between devices, in_one_piece(): lax.all_gather(both, axis, axis=dim, tiled=True)  22.7 us
    all_gather x1, blocking collectives, token_mixer(): lax.all_gather(attended, 'tp', axis=1, tiled=True)  17.4 us
    all_to_all x1, starting transfers between devices, routed_experts(): lax.all_to_all(outgoing, 'ep', split_axis=0, concat_axis=0, tiled=True)  13.8 us
    all_to_all x1, starting transfers between devices, summed_on_arrival(): pieces = lax.all_to_all(cut_along(x, dim, devices), axis, 0, 0, tiled=True)  9.76 us
    all_to_all x1, waiting for transfers between devices, summed_on_arrival(): pieces = lax.all_to_all(cut_along(x, dim, devices), axis, 0, 0, tiled=True)  7.5 us
    all_to_all x1, starting transfers between devices, finish_expert(): return lax.all_to_all(summed, 'ep', split_axis=0, concat_axis=0, tiled=True)  5.23 us
    another operation x2, local copies, waits for them, and re-layouts  4.1 us
  transfers between devices with their start and end apart: 4, of which 3 were waited for; matrix products, arithmetic and copies ran while one was open for 16% of the time, Pallas kernels for 0%

commit v1 on v0

v1 whole, which is shorter than its diff:
```python
import functools

import jax
import jax.numpy as jnp
from jax import lax
from jax.experimental import pallas as pl
from jax.experimental.pallas import tpu as pltpu
from jax.sharding import PartitionSpec as P

MESH = pl.DeviceIdType.MESH
F32 = jnp.float32
BF16 = jnp.bfloat16

NZ, NX, NY = 8, 4, 8
NEP = NZ * NX
D = 2048
HD = 128
ROWS = 128
CAP = 16
SLOTS = NEP * CAP
EPS = 1e-06
DZ_ORDER = (0, 1, 7, 2, 6, 3, 5, 4)
ORDER = "EAEAEAEAEAEAEAEAEAEAEAEAEAEA"


def dot(a, b, dims=((1,), (0,))):
    return lax.dot_general(a, b, (dims, ((), ())), preferred_element_type=F32)


def rdma(src, dst, send_sem, recv_sem, to):
    return pltpu.make_async_remote_copy(
        src_ref=src,
        dst_ref=dst,
        send_sem=send_sem,
        recv_sem=recv_sem,
        device_id=to,
        device_id_type=MESH,
    )


class Ring:
    def __init__(self, n, me, view, half, device_of, sems):
        self.n, self.me, self.view, self.half = n, me, view, half
        self.right = device_of(lax.rem(me + 1, n))
        self.left = device_of(lax.rem(me + n - 1, n))
        self.sems = sems
        self.copies = {}

    def send(self, s):
        n = self.n
        at_r = lax.rem(self.me + n - s, n)
        at_l = lax.rem(self.me + s, n)
        if s < n // 2 - 1:
            ref_r, ref_l = self.view(at_r), self.view(at_l)
        else:
            ref_r, ref_l = self.half(at_r, 0), self.half(at_l, 1)
        sr, rr, sl, rl = self.sems
        r = rdma(ref_r, ref_r, sr.at[s], rr.at[s], self.right)
        l = rdma(ref_l, ref_l, sl.at[s], rl.at[s], self.left)
        r.start()
        l.start()
        self.copies[s] = (r, l)

    def wait(self, s):
        for copy in self.copies[s]:
            copy.wait_recv()

    def drain(self):
        for pair in self.copies.values():
            for copy in pair:
                copy.wait_send()


def mega(
    off_s,
    xa_h, ga_h, wq_h, wk_h, wv_h, wo_h, xb_h, gb_h, ids_h, rw_h, wg_h, wu_h, wd_h,
    out_a, out_b,
    xa, ga, wqkv, wo, xb, gb, ids, rw, wgu, wd,
    na, q, kg, vg, wts, cum, suf, att,
    pk, pt, wth, wtl, xg, acc, po, tosend, fromp, sbr, sbl, rbr, rbl, res, ret,
    in_sem, a2a_s, a2a_r, back_s, back_r,
    kx_sem, kz_sem, vz_sem, vx_sem, at_sem, atp_s, atp_r,
    yg_sem, ygp_s, ygp_r, ex_s, ex_r, rs_sem,
):
    ep = lax.axis_index("ep")
    tp = lax.axis_index("tp")
    z, x = lax.div(ep, NX), lax.rem(ep, NX)
    y, c = lax.div(tp, 2), lax.rem(tp, 2)
    other = 1 - c

    def device(zz, xx, yy, cc):
        return (zz * NX + xx, yy * 2 + cc)

    partner = device(z, x, y, other)
    my_cols = pl.ds(pl.multiple_of(c * HD, HD), HD)

    loads = []

    def load(src, dst):
        copy = pltpu.make_async_copy(src, dst, in_sem.at[len(loads)])
        copy.start()
        loads.append(copy)
        return copy

    l_xb = load(xb_h, xb)
    l_ids = load(ids_h, ids)
    l_gb = load(gb_h, gb)
    l_xa = load(xa_h, xa)
    l_ga = load(ga_h, ga)
    l_qkv = [load(w, wqkv.at[:, pl.ds(i * HD, HD)]) for i, w in enumerate((wq_h, wk_h, wv_h))]
    l_gu = [load(w, wgu.at[:, pl.ds(i * HD, HD)]) for i, w in enumerate((wg_h, wu_h))]
    l_rw = load(rw_h, rw)
    l_wd = load(wd_h, wd)
    l_wo = load(wo_h, wo)

    barrier = pltpu.get_barrier_semaphore()

    def peer(slot, sign):
        dz = DZ_ORDER[slot // NX]
        dx = slot % NX
        if sign > 0:
            return lax.rem(z + dz, NZ), lax.rem(x + dx, NX)
        return lax.rem(z + (NZ - dz), NZ), lax.rem(x + (NX - dx), NX)

    greet = [partner]
    greet.append(device(z, x, lax.rem(y + 1, NY), c))
    greet.append(device(z, x, lax.rem(y + NY - 1, NY), c))
    for slot in range(NEP - 1, 0, -1):
        zz, xx = peer(slot, 1)
        greet.append(device(zz, xx, y, c))
    for to in greet:
        pl.semaphore_signal(barrier, inc=1, device_id=to, device_id_type=MESH)

    l_ids.wait()
    expert = lax.broadcasted_iota(jnp.int32, (NEP, ROWS), 0)
    first = (expert == ids[0:1, :]).astype(F32)
    second = (expert == ids[1:2, :]).astype(F32)
    both = first + second
    earlier = (
        lax.broadcasted_iota(jnp.int32, (ROWS, ROWS), 0)
        < lax.broadcasted_iota(jnp.int32, (ROWS, ROWS), 1)
    ).astype(BF16)
    place = dot(both.astype(BF16), earlier)
    code = jnp.where(both > 0.5, place, 100.0).astype(BF16)
    line = lax.broadcasted_iota(jnp.int32, (SLOTS, NEP), 0)
    slot_i = lax.shift_right_logical(line, 4)
    step_i = lax.shift_right_logical(slot_i, 2)
    odd = (step_i & 1) == 1
    dz_i = jnp.where(
        odd, lax.shift_right_logical(step_i + 1, 1), (NZ - lax.shift_right_logical(step_i, 1))
    )
    to_z = (z + dz_i) & (NZ - 1)
    to_x = (x + (slot_i & (NX - 1))) & (NX - 1)
    spread = (
        (to_z * NX + to_x) == lax.broadcasted_iota(jnp.int32, (SLOTS, NEP), 1)
    ).astype(BF16)
    wanted = (lax.broadcasted_iota(jnp.int32, (SLOTS, ROWS), 0) & (CAP - 1)).astype(F32)
    pick = dot(spread, code) == wanted
    pt[...] = jnp.where(pick, 1.0, 0.0).astype(BF16)

    l_xb.wait()
    l_gb.wait()
    here = pl.ds(pl.multiple_of(tp * HD, HD), HD)
    squares = []
    for r in range(0, ROWS, 16):
        v = xb[pl.ds(r, 16), :].astype(F32)
        squares.append(jnp.sum(v * v, axis=1, keepdims=True))
    mean = jnp.concatenate(squares, axis=0) * (1.0 / D)
    normed = (xb[:, here].astype(F32) * lax.rsqrt(mean + EPS) * gb[:, here]).astype(BF16)
    packed = dot(pt[...], normed).astype(BF16)
    pk[...] = packed
    xg[y, pl.ds(0, CAP), my_cols] = packed[0:CAP, :]

    pl.semaphore_wait(barrier, len(greet))

    a2a = {}
    for slot in range(1, NEP):
        zz, xx = peer(slot, 1)
        rows = pl.ds(slot * CAP, CAP)
        a2a[slot] = rdma(
            pk.at[rows, :], xg.at[y, rows, my_cols], a2a_s.at[slot], a2a_r.at[slot],
            device(zz, xx, y, c),
        )
        a2a[slot].start()

    drains = []

    def attention():
        l_xa.wait()
        l_ga.wait()
        for r in range(0, ROWS, 16):
            v = xa[pl.ds(r, 16), :].astype(F32)
            m = jnp.sum(v * v, axis=1, keepdims=True) * (1.0 / D)
            na[pl.ds(r, 16), :] = (v * lax.rsqrt(m + EPS) * ga[...]).astype(BF16)
        for copy in l_qkv:
            copy.wait()
        qkv = dot(na[...], wqkv[...])
        q[...] = qkv[:, 0:HD].astype(BF16)
        own_k = pl.ds(pl.multiple_of(ep * ROWS, ROWS), ROWS)
        own_v = pl.ds(pl.multiple_of((x * NZ + z) * ROWS, ROWS), ROWS)
        kg[own_k, :] = qkv[:, HD : 2 * HD].astype(BF16)
        vg[own_v, :] = qkv[:, 2 * HD : 3 * HD].astype(BF16)

        def k_rows(block, at, count):
            return kg.at[pl.ds(pl.multiple_of(block * ROWS + at, 16), count), :]

        def v_rows(block, at, count):
            return vg.at[pl.ds(pl.multiple_of(block * ROWS + at, 16), count), :]

        kx = Ring(
            NX, x,
            lambda p: k_rows(z * NX + p, 0, ROWS),
            lambda p, h: k_rows(z * NX + p, h * 64, 64),
            lambda p: device(z, p, y, c),
            [s.at[0] for s in kx_sem],
        )
        kz = [
            Ring(
                NZ, z,
                lambda p, i=i: k_rows(p * NX, i * 256, 256),
                lambda p, h, i=i: k_rows(p * NX, i * 256 + h * 128, 128),
                lambda p: device(p, x, y, c),
                [s.at[i] for s in kz_sem],
            )
            for i in range(2)
        ]
        vz = Ring(
            NZ, z,
            lambda p: v_rows(x * NZ + p, 0, ROWS),
            lambda p, h: v_rows(x * NZ + p, h * 64, 64),
            lambda p: device(p, x, y, c),
            [s.at[0] for s in vz_sem],
        )
        vx = [
            Ring(
                NX, x,
                lambda p, i=i: v_rows(p * NZ, i * 512, 512),
                lambda p, h, i=i: v_rows(p * NZ, i * 512 + h * 256, 256),
                lambda p: device(z, p, y, c),
                [s.at[i] for s in vx_sem],
            )
            for i in range(2)
        ]
        drains.extend([kx, *kz, vz, *vx])
        kx.send(0)
        vz.send(0)
        yield

        j = lax.broadcasted_iota(jnp.int32, (256, 256), 0) & (ROWS - 1)
        s = lax.broadcasted_iota(jnp.int32, (256, 256), 1)
        suf[...] = jnp.where((j > s) | (s >= ROWS), 1.0, 0.0).astype(BF16)
        cum[...] = jnp.zeros_like(cum)
        q_pos = ep * ROWS + lax.broadcasted_iota(jnp.int32, (ROWS, 512), 0)
        k_off = lax.broadcasted_iota(jnp.int32, (ROWS, 512), 1)

        def group(d):
            g = lax.rem(z + (NZ - d), NZ)
            keys = kg[pl.ds(pl.multiple_of(g * 512, 512), 512), :]
            zf = dot(q[...], keys, ((1,), (1,))) * (HD ** -0.5) + off_s[0]
            causal = (k_off + g * 512) < q_pos
            soft = jnp.maximum(zf, 0.0) + jnp.log(1.0 + jnp.exp(-jnp.abs(zf)))
            keep = jnp.where(causal, -soft, 0.0)
            later = cum[...]
            for b in range(NX - 1, -1, -1):
                cut = slice(b * ROWS, (b + 1) * ROWS)
                kb = keep[:, cut]
                high = kb.astype(BF16)
                low = (kb - high.astype(F32)).astype(BF16)
                sums = dot(jnp.concatenate([high, low], axis=1), suf[...])
                arg = zf[:, cut] + kb + sums[:, :ROWS] + later
                w = jnp.where(causal[:, cut], jnp.exp(arg), 0.0).astype(BF16)
                at = pl.multiple_of((b * NZ + g) * ROWS, ROWS)
                wts[:, pl.ds(at, ROWS)] = w
                later = later + sums[:, ROWS:]
            cum[...] = later

        kx.wait(0)
        kx.send(1)
        vz.wait(0)
        vz.send(1)
        yield
        kx.wait(1)
        for r in kz:
            r.send(0)
        group(0)
        yield
        vz.wait(1)
        vz.send(2)
        yield
        for s_at in range(3):
            for r in kz:
                r.wait(s_at)
                r.send(s_at + 1)
            group(s_at + 1)
            yield
            if s_at == 0:
                vz.wait(2)
                vz.send(3)
                yield
            if s_at == 1:
                vz.wait(3)
                for r in vx:
                    r.send(0)
                yield
            if s_at == 2:
                for r in vx:
                    r.wait(0)
                    r.send(1)
                yield
        for r in kz:
            r.wait(3)

        @pl.loop(4, 8)
        def _(d):
            group(d)

        yield
        for r in vx:
            r.wait(1)
        attended = dot(wts[...], vg[...]).astype(BF16)
        att[y, :, my_cols] = attended
        ring = Ring(
            NY, y,
            lambda p: att.at[p, :, my_cols],
            lambda p, h: att.at[p, pl.ds(h * 64, 64), my_cols],
            lambda p: device(z, x, p, c),
            [s.at[0] for s in at_sem],
        )
        drains.append(ring)
        across = []

        def hand_over(i):
            p = lax.rem(y + (NY - i), NY)
            ref = att.at[p, :, my_cols]
            copy = rdma(ref, ref, atp_s.at[i], atp_r.at[i], partner)
            copy.start()
            across.append(copy)

        ring.send(0)
        hand_over(0)
        yield
        for s_at in range(4):
            ring.wait(s_at)
            if s_at < 3:
                ring.send(s_at + 1)
                hand_over(s_at + 1)
                hand_over(7 - s_at)
            else:
                hand_over(4)
            yield
        for copy in across:
            copy.wait_recv()
        l_wo.wait()
        total = dot(att[0], wo[pl.ds(0, 256), :])
        for i in range(1, NY):
            total += dot(att[i], wo[pl.ds(i * 256, 256), :])
        out_a[...] = total.astype(BF16)
        for copy in across:
            copy.wait_send()
        yield

    def experts():
        yg = [
            Ring(
                NY, y,
                lambda p, h=h: xg.at[p, pl.ds(h * 256, 256), my_cols],
                lambda p, k, h=h: xg.at[p, pl.ds(h * 256 + k * 128, 128), my_cols],
                lambda p: device(z, x, p, c),
                [s.at[h] for s in yg_sem],
            )
            for h in range(2)
        ]
        drains.extend(yg)
        across = {}

        def hand_over(h, i):
            p = lax.rem(y + (NY - i), NY)
            ref = xg.at[p, pl.ds(h * 256, 256), my_cols]
            copy = rdma(ref, ref, ygp_s.at[h, i], ygp_r.at[h, i], partner)
            copy.start()
            across[h, i] = copy

        for h in range(2):
            for slot in range(h * 16, h * 16 + 16):
                if slot > 0:
                    a2a[slot].wait_recv()
            yg[h].send(0)
            hand_over(h, 0)
        yield
        for copy in l_gu:
            copy.wait()

        def multiply(i, start=False):
            for h in range(2):
                across[h, i].wait_recv()
            p = lax.rem(y + (NY - i), NY)
            part = dot(xg[p], wgu[pl.ds(pl.multiple_of(p * 256, 256), 256), :])
            if start:
                acc[...] = part
            else:
                acc[...] += part

        for s_at in range(4):
            for h in range(2):
                yg[h].wait(s_at)
                if s_at < 3:
                    yg[h].send(s_at + 1)
                    hand_over(h, s_at + 1)
                    hand_over(h, 7 - s_at)
                else:
                    hand_over(h, 4)
            if s_at == 0:
                multiply(0, True)
            else:
                multiply(s_at)
                multiply(8 - s_at)
            yield
        multiply(4)
        gate, up = acc[:, 0:HD], acc[:, HD : 2 * HD]
        hidden = (gate / (1.0 + jnp.exp(-gate)) * up).astype(BF16)
        l_wd.wait()
        trades = {}
        for i in (4, 3, 5, 2, 6, 1, 7, 0):
            p = lax.rem(y + i, NY)
            part = dot(hidden, wd[:, pl.ds(pl.multiple_of(p * 256, 256), 256)])
            lower, upper = part[:, 0:HD], part[:, HD : 2 * HD]
            po[i] = jnp.where(c == 0, lower, upper)
            tosend[i] = jnp.where(c == 0, upper, lower).astype(BF16)
            trades[i] = rdma(tosend.at[i], fromp.at[i], ex_s.at[i], ex_r.at[i], partner)
            trades[i].start()
        yield
        right = device(z, x, lax.rem(y + 1, NY), c)
        left = device(z, x, lax.rem(y + NY - 1, NY), c)
        moved = []
        last = {}
        for s_at in range(4):
            i_r, i_l = 4 - s_at, 4 + s_at
            trades[i_r].wait_recv()
            if i_l != i_r:
                trades[i_l].wait_recv()
            for h in range(2):
                base = h * 256
                if s_at == 0:
                    spans_r, spans_l = ((0, 128, False),), ((128, 128, False),)
                elif s_at == 1:
                    spans_r = ((0, 128, True), (128, 128, False))
                    spans_l = ((0, 128, False), (128, 128, True))
                else:
                    spans_r = spans_l = ((0, 256, True),)
                for way, i, spans, sent, got, to, sems in (
                    (0, i_r, spans_r, sbr, rbr, right, (rs_sem[0], rs_sem[1])),
                    (1, i_l, spans_l, sbl, rbl, left, (rs_sem[2], rs_sem[3])),
                ):
                    if s_at > 0:
                        last[way, h].wait_recv()
                    for at, count, add in spans:
                        rows = pl.ds(base + at, count)
                        value = po[i, rows, :] + fromp[i, rows, :].astype(F32)
                        if add:
                            value = value + got[s_at - 1, rows, :].astype(F32)
                        sent[s_at, rows, :] = value.astype(BF16)
                    lo = spans[0][0]
                    n = sum(span[1] for span in spans)
                    rows = pl.ds(base + lo, n)
                    copy = rdma(
                        sent.at[s_at, rows, :], got.at[s_at, rows, :],
                        sems[0].at[h, s_at], sems[1].at[h, s_at], to,
                    )
                    copy.start()
                    moved.append(copy)
                    last[way, h] = copy
            yield
        trades[0].wait_recv()
        back = {}
        for h in range(2):
            last[0, h].wait_recv()
            last[1, h].wait_recv()
            rows = pl.ds(h * 256, 256)
            value = po[0, rows, :] + fromp[0, rows, :].astype(F32)
            value = value + rbr[3, rows, :].astype(F32) + rbl[3, rows, :].astype(F32)
            res[rows, :] = value.astype(BF16)
            if h == 0:
                ret[pl.ds(0, CAP), :] = value[0:CAP, :].astype(BF16)
            for slot in range(h * 16, h * 16 + 16):
                if slot > 0:
                    zz, xx = peer(slot, -1)
                    at = pl.ds(slot * CAP, CAP)
                    back[slot] = rdma(
                        res.at[at, :], ret.at[at, :], back_s.at[slot], back_r.at[slot],
                        device(zz, xx, y, c),
                    )
                    back[slot].start()
        l_rw.wait()
        weight = first * rw[0:1, :] + second * rw[1:2, :]
        w_high = weight.astype(BF16)
        w_low = (weight - w_high.astype(F32)).astype(BF16)
        mask = pt[...].astype(F32)
        wth[...] = (dot(spread, w_high) * mask).astype(BF16)
        wtl[...] = (dot(spread, w_low) * mask).astype(BF16)
        yield
        for slot in range(1, NEP):
            back[slot].wait_recv()
        over_slots = ((0,), (0,))
        combined = dot(wth[...], ret[...], over_slots) + dot(wtl[...], ret[...], over_slots)
        out_b[...] = combined.astype(BF16)
        for copy in (*across.values(), *trades.values(), *moved, *back.values()):
            copy.wait_send()
        yield

    halves = {"E": experts(), "A": attention()}
    for name in ORDER:
        if name in halves:
            try:
                next(halves[name])
            except StopIteration:
                del halves[name]
    for rest in halves.values():
        for _ in rest:
            pass
    for copy in a2a.values():
        copy.wait_send()
    for ring in drains:
        ring.drain()


def ring_sems(count, steps):
    return [pltpu.SemaphoreType.DMA((count, steps))] * 4


def on_device(
    mixer_input, mixer_gain, query_weight, key_weight, value_weight, score_offset, out_weight,
    expert_input, expert_gain, route_ids, route_weights, gate_weight, up_weight, down_weight,
):
    hbm = pl.BlockSpec(memory_space=pl.ANY)
    vmem = pl.BlockSpec(memory_space=pltpu.VMEM)
    dma = pltpu.SemaphoreType.DMA
    out = jax.ShapeDtypeStruct((ROWS, HD), BF16)
    scratch = [
        pltpu.VMEM((ROWS, D), BF16),
        pltpu.VMEM((1, D), F32),
        pltpu.VMEM((D, 3 * HD), BF16),
        pltpu.VMEM((D, HD), BF16),
        pltpu.VMEM((ROWS, D), BF16),
        pltpu.VMEM((1, D), F32),
        pltpu.VMEM((2, ROWS), jnp.int32),
        pltpu.VMEM((2, ROWS), F32),
        pltpu.VMEM((D, 2 * HD), BF16),
        pltpu.VMEM((HD, D), BF16),
        pltpu.VMEM((ROWS, D), BF16),
        pltpu.VMEM((ROWS, HD), BF16),
        pltpu.VMEM((NEP * ROWS, HD), BF16),
        pltpu.VMEM((NEP * ROWS, HD), BF16),
        pltpu.VMEM((ROWS, NEP * ROWS), BF16),
        pltpu.VMEM((ROWS, ROWS), F32),
        pltpu.VMEM((256, 256), BF16),
        pltpu.VMEM((NY, ROWS, 2 * HD), BF16),
        pltpu.VMEM((SLOTS, HD), BF16),
        pltpu.VMEM((SLOTS, ROWS), BF16),
        pltpu.VMEM((SLOTS, ROWS), BF16),
        pltpu.VMEM((SLOTS, ROWS), BF16),
        pltpu.VMEM((NY, SLOTS, 2 * HD), BF16),
        pltpu.VMEM((SLOTS, 2 * HD), F32),
        pltpu.VMEM((NY, SLOTS, HD), F32),
        pltpu.VMEM((NY, SLOTS, HD), BF16),
        pltpu.VMEM((NY, SLOTS, HD), BF16),
        pltpu.VMEM((4, SLOTS, HD), BF16),
        pltpu.VMEM((4, SLOTS, HD), BF16),
        pltpu.VMEM((4, SLOTS, HD), BF16),
        pltpu.VMEM((4, SLOTS, HD), BF16),
        pltpu.VMEM((SLOTS, HD), BF16),
        pltpu.VMEM((SLOTS, HD), BF16),
        dma((13,)),
        dma((NEP,)), dma((NEP,)), dma((NEP,)), dma((NEP,)),
        ring_sems(1, 2), ring_sems(2, 4), ring_sems(1, 4), ring_sems(2, 2),
        ring_sems(1, 4), dma((NY,)), dma((NY,)),
        ring_sems(2, 4), dma((2, NY)), dma((2, NY)),
        dma((NY,)), dma((NY,)), ring_sems(2, 4),
    ]
    flat, tree = jax.tree.flatten(scratch)

    def body(*refs):
        fixed = 1 + 13 + 2
        mega(*refs[:fixed], *jax.tree.unflatten(tree, refs[fixed:]))

    mixed, routed = pl.pallas_call(
        body,
        out_shape=(out, out),
        in_specs=[pl.BlockSpec(memory_space=pltpu.SMEM)] + [hbm] * 13,
        out_specs=(vmem, vmem),
        scratch_shapes=flat,
        compiler_params=pltpu.CompilerParams(
            collective_id=0, has_side_effects=True, vmem_limit_bytes=60 * 1024 * 1024
        ),
        name="both_halves",
    )(
        score_offset,
        mixer_input, mixer_gain.reshape(1, D), query_weight, key_weight, value_weight, out_weight,
        expert_input, expert_gain.reshape(1, D), route_ids.T, route_weights.T,
        gate_weight.reshape(D, HD), up_weight.reshape(D, HD), down_weight.reshape(HD, D),
    )
    return mixed, routed


def solution(mesh):
    in_specs = (
        P("ep", None),
        P(),
        P(None, "tp"),
        P(None, "tp"),
        P(None, "tp"),
        P("tp"),
        P(None, "tp"),
        P("ep", None),
        P(),
        P("ep", None),
        P("ep", None),
        P("ep", None, "tp"),
        P("ep", None, "tp"),
        P("ep", "tp", None),
    )
    out_specs = (P("ep", "tp"), P("ep", "tp"))
    return jax.shard_map(
        on_device, mesh=mesh, in_specs=in_specs, out_specs=out_specs, check_vma=False
    )
```

time: 180 us -> 89.7 us (0.50)
  Pallas kernels: 0 us -> 86.2 us
  waiting for transfers between devices: 77.3 us -> 0 us
  starting transfers between devices: 28.9 us -> 0 us
  blocking collectives: 17.4 us -> 0 us
  matrix products: 13.2 us -> 0 us
  other arithmetic: 13.2 us -> 0 us
  local copies, waits for them, and re-layouts: 15 us -> 2 us
  between operations: 14.2 us -> 1.3 us
    pallas_call x0 -> x1, Pallas kernels: none -> 86.2 us  [on_device(): pl.pallas_call(body, out_shape=(out, out), in_specs=[pl.BlockSpec(memory_...]
    all_to_all x3 -> x0, waiting for transfers between devices: 54.6 us -> none  [the longest x1 47.1 us: routed_experts(): lax.all_to_all(outgoing, 'ep', split_axis=0, concat_axis=0, tiled=True)]
    all_to_all x3 -> x0, starting transfers between devices: 28.8 us -> none  [the longest x1 13.8 us: routed_experts(): lax.all_to_all(outgoing, 'ep', split_axis=0, concat_axis=0, tiled=True)]
    all_gather x1 -> x0, waiting for transfers between devices: 22.7 us -> none  [in_one_piece(): lax.all_gather(both, axis, axis=dim, tiled=True)]
    all_gather x1 -> x0, blocking collectives: 17.4 us -> none  [token_mixer(): lax.all_gather(attended, 'tp', axis=1, tiled=True)]
    dot_general x10 -> x0, matrix products: 13.2 us -> none  [the longest x1 2.57 us: attend_set(): jnp.einsum('qhd,bkhd->bhqk', query_heads, key_heads, preferred_element_ty...]
    reduce_sum x7 -> x0, other arithmetic: 5.38 us -> none  [the longest x1 1.98 us: token_mixer(): summed = jnp.sum(jnp.exp(later_keep)[..., None] * block_out, axis=0)]
    convert_element_type x3 -> x0, other arithmetic: 5.22 us -> none  [the longest x1 3.98 us: attend_set(): jnp.where(causal, jnp.exp(jax.nn.log_sigmoid(scores) + after_sum), 0.0)]
  transfers between devices with their start and end apart: 4 -> 0, of which waited for: 3 -> 0; matrix products, arithmetic and copies ran while one was open for 16% -> 0% of each run, Pallas kernels for 0% -> 0%
where the time goes in v1:
time: 89.7 us; the launch traced here: 89.5 us
  Pallas kernels  86.2 us (96%)
  local copies, waits for them, and re-layouts  2 us (2%)
  between operations  1.3 us (1%)
    pallas_call x1, Pallas kernels, on_device(): pl.pallas_call(body, out_shape=(out, out), in_specs=[pl.BlockSpec(memory_...  86.2 us
    unnamed x4, local copies, waits for them, and re-layouts  2 us

profile of v1, /device:TPU:1, one launch (start us, length us, event | category | flops | bytes accessed | tf_op | source)
XLA Modules:
  0.0 89.5 jit_solution(10560713975702083437)
XLA Ops:
  1.3 86.2 %both_halves.1 = (bf16[128,128]{1,0:T(8,128)(2,1)}, bf16[128,128]{1,0:T(8,128)(2,1)}) custom-call(f32[1]{0:T(128)S(6)} %copy.18.refs_0_, bf16[128,2048]{1,0:T(8,128)(2,1)} %refs_1_.1, f32[1,2048]{1,0:T(1,128)} %bitcast.10, bf16[2048,128]{1,0:T(8,128)(2,1)} %refs_3_.1, bf16[2048,128]{1,0:T(8,128)(2,1)} %refs_4_.1, bf16[2048,128]{1,0:T(8,128)(2,1)} %refs_5_.1, ...), custom_call_target="tpu_custom_call" | custom-call | tf_op jit(solution)/shard_map/both_halves/pallas_call | solution.py:585
  87.5 0.0 copy-start
  87.5 1.4 %copy.19 = bf16[128,128]{1,0:T(8,128)(2,1)} copy(bf16[128,128]{1,0:T(8,128)(2,1)} %get-tuple-element.4) | data formatting | bytes 65536
  88.9 0.0 copy-done
  88.9 0.6 copy.20
Async XLA Ops:
  87.5 1.4 %copy-start = (bf16[128,128]{1,0:T(8,128)(2,1)S(1)}, bf16[128,128]{1,0:T(8,128)(2,1)}, u32[]{:S(2)}) copy-start(bf16[128,128]{1,0:T(8,128)(2,1)} %get-tuple-element.5) | copy-start | bytes 98308

commit v2 on v1

v2 whole, which is shorter than its diff:
```python
import functools

import jax
import jax.numpy as jnp
from jax import lax
from jax.experimental import pallas as pl
from jax.experimental.pallas import tpu as pltpu
from jax.sharding import PartitionSpec as P

MESH = pl.DeviceIdType.MESH
F32 = jnp.float32
BF16 = jnp.bfloat16

NZ, NX, NY = 8, 4, 8
NEP = NZ * NX
D = 2048
HD = 128
ROWS = 128
CAP = 16
SLOTS = NEP * CAP
EPS = 1e-06
DZ_ORDER = (0, 1, 7, 2, 6, 3, 5, 4)
PART = 128
PARTS = SLOTS // PART
ORDER = "".join(
    (
        "VKD0K12V30123KK01K23K0KV",
        "1K0213KK0213KK230KV1KK2W",
        "3V0K1KK2K3K0K1VO23O1023O",
        "OC",
    )
)


def dot(a, b, dims=((1,), (0,))):
    return lax.dot_general(a, b, (dims, ((), ())), preferred_element_type=F32)


def rdma(src, dst, send_sem, recv_sem, to):
    return pltpu.make_async_remote_copy(
        src_ref=src,
        dst_ref=dst,
        send_sem=send_sem,
        recv_sem=recv_sem,
        device_id=to,
        device_id_type=MESH,
    )


class Ring:
    def __init__(self, name, n, me, view, half, device_of, sems):
        self.name = name
        self.n, self.me, self.view, self.half = n, me, view, half
        self.right = device_of(lax.rem(me + 1, n))
        self.left = device_of(lax.rem(me + n - 1, n))
        self.sems = sems
        self.copies = {}

    def send(self, s):
        n = self.n
        at_r = lax.rem(self.me + n - s, n)
        at_l = lax.rem(self.me + s, n)
        if self.half is None or s < n // 2 - 1:
            ref_r, ref_l = self.view(at_r), self.view(at_l)
        else:
            ref_r, ref_l = self.half(at_r, 0), self.half(at_l, 1)
        sr, rr, sl, rl = self.sems
        r = rdma(ref_r, ref_r, sr.at[s], rr.at[s], self.right)
        l = rdma(ref_l, ref_l, sl.at[s], rl.at[s], self.left)
        r.start()
        l.start()
        self.copies[s] = (r, l)

    def wait(self, s):
        with jax.named_scope(f"{self.name}_wait#s={s}"):
            for copy in self.copies[s]:
                copy.wait_recv()

    def drain(self):
        for pair in self.copies.values():
            for copy in pair:
                copy.wait_send()


class TwoStage:
    PLAN = (
        (0, 0, 2, 2), (0, 0, 2, -2), (0, 0, 2, 1), (0, 0, 2, -1),
        (-2, 0, 1, 2), (-2, 0, 2, 1), (2, 1, 2, -2), (2, 0, 2, -1),
    )

    def __init__(self, name, me, rows, view, device_of, sems):
        self.name, self.me, self.rows = name, me, rows
        self.view, self.device_of, self.sems = view, device_of, sems
        self.copies = {}

    def place(self, offset):
        return lax.rem(self.me + 8 + offset, 8)

    def send(self, i):
        block, first, last, to = self.PLAN[i]
        half = self.rows // 2
        ref = self.view(self.place(block), first * half, (last - first) * half)
        copy = rdma(
            ref, ref, self.sems[0].at[i], self.sems[1].at[i], self.device_of(self.place(to))
        )
        copy.start()
        self.copies[i] = copy

    def start(self):
        for i in range(4):
            self.send(i)

    def wait(self, *which):
        with jax.named_scope(f"{self.name}_wait#s={which[0]}"):
            for i in which:
                self.copies[i].wait_recv()

    def drain(self):
        for copy in self.copies.values():
            copy.wait_send()


def mega(
    off_h,
    xa_h, ga_h, wq_h, wk_h, wv_h, wo_h, xb_h, gb_h, ids_h, rw_h, wg_h, wu_h, wd_h,
    out_ab,
    off, xa, ga, wqkv, wo, xb, gb, ids, rw, wgu, wd,
    na, q, kg, vg, wts, cum, suf, att,
    pk, pt, wth, wtl, xg, acc, po, tosend, fromp, sbr, sbl, rbr, rbl, res, ret,
    in_sem, a2a_s, a2a_r, back_s, back_r,
    kx_s, kx_r, kz_sem, vz_s, vz_r, vx_sem, at_s, at_r, atp_s, atp_r,
    yg_sem, ygp_s, ygp_r, ex_s, ex_r, rs_sem,
):
    ep = lax.axis_index("ep")
    tp = lax.axis_index("tp")
    z, x = lax.div(ep, NX), lax.rem(ep, NX)
    y, c = lax.div(tp, 2), lax.rem(tp, 2)
    other = 1 - c

    def device(zz, xx, yy, cc):
        return (zz * NX + xx, yy * 2 + cc)

    partner = device(z, x, y, other)
    my_cols = pl.ds(pl.multiple_of(c * HD, HD), HD)

    loads = []

    def load(src, dst):
        copy = pltpu.make_async_copy(src, dst, in_sem.at[len(loads)])
        copy.start()
        loads.append(copy)
        return copy

    l_xb = load(xb_h, xb)
    l_ids = load(ids_h, ids)
    l_gb = load(gb_h, gb)
    l_xa = load(xa_h, xa)
    l_ga = load(ga_h, ga)
    l_qkv = [load(w, wqkv.at[:, pl.ds(i * HD, HD)]) for i, w in enumerate((wq_h, wk_h, wv_h))]
    l_gu = [load(w, wgu.at[:, pl.ds(i * HD, HD)]) for i, w in enumerate((wg_h, wu_h))]
    l_rw = load(rw_h, rw)
    l_wd = load(wd_h, wd)
    l_wo = load(wo_h, wo)
    l_off = load(off_h, off)

    barrier = pltpu.get_barrier_semaphore()

    def peer(slot, sign):
        dz = DZ_ORDER[slot // NX]
        dx = slot % NX
        if sign > 0:
            return lax.rem(z + dz, NZ), lax.rem(x + dx, NX)
        return lax.rem(z + (NZ - dz), NZ), lax.rem(x + (NX - dx), NX)

    greet = [partner]
    greet.append(device(z, x, lax.rem(y + 1, NY), c))
    greet.append(device(z, x, lax.rem(y + NY - 1, NY), c))
    for slot in range(NEP - 1, 0, -1):
        zz, xx = peer(slot, 1)
        greet.append(device(zz, xx, y, c))
    for to in greet:
        pl.semaphore_signal(barrier, inc=1, device_id=to, device_id_type=MESH)

    l_ids.wait()
    expert = lax.broadcasted_iota(jnp.int32, (NEP, ROWS), 0)
    first = (expert == ids[0:1, :]).astype(F32)
    second = (expert == ids[1:2, :]).astype(F32)
    both = first + second
    earlier = (
        lax.broadcasted_iota(jnp.int32, (ROWS, ROWS), 0)
        < lax.broadcasted_iota(jnp.int32, (ROWS, ROWS), 1)
    ).astype(BF16)
    place = dot(both.astype(BF16), earlier)
    code = jnp.where(both > 0.5, place, 100.0).astype(BF16)
    line = lax.broadcasted_iota(jnp.int32, (SLOTS, NEP), 0)
    slot_i = lax.shift_right_logical(line, 4)
    step_i = lax.shift_right_logical(slot_i, 2)
    odd = (step_i & 1) == 1
    dz_i = jnp.where(
        odd, lax.shift_right_logical(step_i + 1, 1), (NZ - lax.shift_right_logical(step_i, 1))
    )
    to_z = (z + dz_i) & (NZ - 1)
    to_x = (x + (slot_i & (NX - 1))) & (NX - 1)
    spread = (
        (to_z * NX + to_x) == lax.broadcasted_iota(jnp.int32, (SLOTS, NEP), 1)
    ).astype(BF16)
    wanted = (lax.broadcasted_iota(jnp.int32, (SLOTS, ROWS), 0) & (CAP - 1)).astype(F32)
    pick = dot(spread, code) == wanted
    pt[...] = jnp.where(pick, 1.0, 0.0).astype(BF16)

    with jax.named_scope("xb_wait"):
        l_xb.wait()
        l_gb.wait()
    squares = []
    for r in range(0, ROWS, 16):
        v = xb[pl.ds(r, 16), :].astype(F32)
        squares.append(jnp.sum(v * v, axis=1, keepdims=True))
    mean = jnp.concatenate(squares, axis=0) * (1.0 / D)
    scale = lax.rsqrt(mean + EPS)
    opposite = lax.rem(y + NY // 2, NY)

    def pack(i, chip):
        cols = pl.ds(pl.multiple_of((chip * 2 + c) * HD, HD), HD)
        normed = (xb[:, cols].astype(F32) * scale * gb[:, cols]).astype(BF16)
        packed = dot(pt[...], normed).astype(BF16)
        pk[i] = packed
        xg[chip, pl.ds(0, CAP), my_cols] = packed[0:CAP, :]

    pack(0, y)
    pack(1, opposite)

    drains = []
    order_done = []

    with jax.named_scope("xa_wait"):
        l_xa.wait()
        l_ga.wait()
    for r in range(0, ROWS, 16):
        v = xa[pl.ds(r, 16), :].astype(F32)
        m = jnp.sum(v * v, axis=1, keepdims=True) * (1.0 / D)
        na[pl.ds(r, 16), :] = (v * lax.rsqrt(m + EPS) * ga[...]).astype(BF16)
    with jax.named_scope("qkv_wait"):
        for copy in l_qkv:
            copy.wait()
        l_off.wait()
    qkv = dot(na[...], wqkv[...])
    q[...] = qkv[:, 0:HD].astype(BF16)
    own_k = pl.ds(pl.multiple_of(ep * ROWS, ROWS), ROWS)
    own_v = pl.ds(pl.multiple_of((x * NZ + z) * ROWS, ROWS), ROWS)
    kg[own_k, :] = qkv[:, HD : 2 * HD].astype(BF16)
    vg[own_v, :] = qkv[:, 2 * HD : 3 * HD].astype(BF16)
    suf_j = lax.broadcasted_iota(jnp.int32, (256, 256), 0) & (ROWS - 1)
    suf_s = lax.broadcasted_iota(jnp.int32, (256, 256), 1)
    suf[...] = jnp.where((suf_j > suf_s) | (suf_s >= ROWS), 1.0, 0.0).astype(BF16)
    cum[...] = jnp.zeros_like(cum)

    with jax.named_scope("barrier_wait"):
        pl.semaphore_wait(barrier, len(greet))

    a2a = {}

    def send_rows(i, chip):
        for slot in range(1, NEP):
            zz, xx = peer(slot, 1)
            rows = pl.ds(slot * CAP, CAP)
            a2a[i, slot] = rdma(
                pk.at[i, rows, :], xg.at[chip, rows, my_cols],
                a2a_s.at[i, slot], a2a_r.at[i, slot], device(zz, xx, y, c),
            )
            a2a[i, slot].start()

    send_rows(0, y)

    def opposite_rows():
        send_rows(1, opposite)
        yield

    q_pos = ep * ROWS + lax.broadcasted_iota(jnp.int32, (ROWS, 512), 0)
    k_off = lax.broadcasted_iota(jnp.int32, (ROWS, 512), 1)

    def group(d):
        with jax.named_scope("group"):
            g = lax.rem(z + (NZ - d), NZ)
            keys = kg[pl.ds(pl.multiple_of(g * 512, 512), 512), :]
            zf = dot(q[...], keys, ((1,), (1,))) * (HD ** -0.5) + off[...]
            causal = (k_off + g * 512) < q_pos
            soft = jnp.maximum(zf, 0.0) + jnp.log(1.0 + jnp.exp(-jnp.abs(zf)))
            keep = jnp.where(causal, -soft, 0.0)
            later = cum[...]
            for b in range(NX - 1, -1, -1):
                cut = slice(b * ROWS, (b + 1) * ROWS)
                kb = keep[:, cut]
                high = kb.astype(BF16)
                low = (kb - high.astype(F32)).astype(BF16)
                sums = dot(jnp.concatenate([high, low], axis=1), suf[...])
                arg = zf[:, cut] + kb + sums[:, :ROWS] + later
                w = jnp.where(causal[:, cut], jnp.exp(arg), 0.0).astype(BF16)
                at = pl.multiple_of((b * NZ + g) * ROWS, ROWS)
                wts[:, pl.ds(at, ROWS)] = w
                later = later + sums[:, ROWS:]
            cum[...] = later

    def key_side():
        def k_rows(block, at, count):
            return kg.at[pl.ds(pl.multiple_of(block * ROWS + at, 16), count), :]

        kx = []
        for j in range(1, NX):
            ref = k_rows(ep, 0, ROWS)
            to = device(z, lax.rem(x + j, NX), y, c)
            kx.append(rdma(ref, ref, kx_s.at[j], kx_r.at[j], to))
        kz = [
            Ring(
                "kz", NZ, z,
                lambda p, j=j: k_rows(p * NX + lax.rem(x + NX - j, NX), 0, ROWS),
                lambda p, h, j=j: k_rows(p * NX + lax.rem(x + NX - j, NX), h * 64, 64),
                lambda p: device(p, x, y, c),
                [s.at[j] for s in kz_sem],
            )
            for j in range(NX)
        ]
        drains.extend(kz)
        for copy in kx:
            copy.start()
        kz[0].send(0)
        yield
        with jax.named_scope("kx_wait"):
            for j in range(1, NX):
                kx[j - 1].wait_recv()
                kz[j].send(0)
        group(0)
        yield
        for s_at in range(4):
            for r in kz:
                r.wait(s_at)
                if s_at < 3:
                    r.send(s_at + 1)
                if r is kz[-1]:
                    group(s_at + 1)
                yield
        for d in (5, 6, 7):
            group(d)
            yield
        for copy in kx:
            copy.wait_send()
        yield

    def value_side():
        def v_rows(block, at, count):
            return vg.at[pl.ds(pl.multiple_of(block * ROWS + at, 16), count), :]

        vz = TwoStage(
            "vz", z, ROWS,
            lambda p, at, count: v_rows(x * NZ + p, at, count),
            lambda p: device(p, x, y, c),
            (vz_s, vz_r),
        )
        vx = [
            Ring(
                "vx", NX, x,
                lambda p, i=i: v_rows(p * NZ, i * 256, 256),
                lambda p, h, i=i: v_rows(p * NZ, i * 256 + h * 128, 128),
                lambda p: device(z, p, y, c),
                [s.at[i] for s in vx_sem],
            )
            for i in range(4)
        ]
        drains.extend([vz, *vx])
        vz.start()
        yield
        vz.wait(0)
        vz.send(5)
        vz.send(4)
        vz.wait(1)
        vz.send(7)
        vz.send(6)
        yield
        vz.wait(2, 3, 4, 5, 6, 7)
        for r in vx:
            r.send(0)
        yield
        for r in vx:
            r.wait(0)
            r.send(1)
            if r is vx[1]:
                yield
        yield
        for r in vx:
            r.wait(1)
        yield

    def out_side():
        assert order_done.count("K") > 20 and order_done.count("V") > 5
        attended = dot(wts[...], vg[...]).astype(BF16)
        att[y, :, my_cols] = attended
        ring = TwoStage(
            "at", y, ROWS,
            lambda p, at, count: att.at[p, pl.ds(at, count), my_cols],
            lambda p: device(z, x, p, c),
            (at_s, at_r),
        )
        drains.append(ring)
        across = []

        def hand_over(i):
            p = lax.rem(y + NY + i, NY)
            ref = att.at[p, :, my_cols]
            copy = rdma(ref, ref, atp_s.at[i + 3], atp_r.at[i + 3], partner)
            copy.start()
            across.append(copy)

        ring.start()
        hand_over(0)
        yield
        ring.wait(0)
        ring.send(5)
        ring.send(4)
        ring.wait(1)
        ring.send(7)
        ring.send(6)
        hand_over(-2)
        hand_over(2)
        ring.wait(2, 3)
        hand_over(-1)
        hand_over(1)
        yield
        ring.wait(5, 7)
        hand_over(-3)
        hand_over(3)
        ring.wait(4, 6)
        hand_over(4)
        yield
        with jax.named_scope("at_pair_wait"):
            for copy in across:
                copy.wait_recv()
        l_wo.wait()
        total = dot(att[0], wo[pl.ds(0, 256), :])
        for i in range(1, NY):
            total += dot(att[i], wo[pl.ds(i * 256, 256), :])
        out_ab[0] = total.astype(BF16)
        for copy in across:
            copy.wait_send()
        yield

    back = {}

    def experts(part_at):
        base = part_at * PART
        yg = Ring(
            "yg", NY, y,
            lambda p: xg.at[p, pl.ds(base, PART), my_cols],
            None,
            lambda p: device(z, x, p, c),
            [s.at[part_at] for s in yg_sem],
        )
        drains.append(yg)
        across = {}

        def hand_over(i):
            p = lax.rem(y + (NY - i), NY)
            ref = xg.at[p, pl.ds(base, PART), my_cols]
            copy = rdma(ref, ref, ygp_s.at[part_at, i], ygp_r.at[part_at, i], partner)
            copy.start()
            across[i] = copy

        slots = range(base // CAP, (base + PART) // CAP)
        with jax.named_scope("a2a_wait"):
            for slot in slots:
                if slot > 0:
                    a2a[0, slot].wait_recv()
        yg.send(0)
        hand_over(0)
        yield
        if part_at == 0:
            for copy in l_gu:
                copy.wait()
            l_wd.wait()
        mine = pl.ds(base, PART)

        def multiply(i, start=False):
            with jax.named_scope("pair_wait"):
                across[i].wait_recv()
            p = lax.rem(y + (NY - i), NY)
            part = dot(xg[p, mine, :], wgu[pl.ds(pl.multiple_of(p * 256, 256), 256), :])
            if start:
                acc[mine, :] = part
            else:
                acc[mine, :] += part

        for s_at in range(3):
            yg.wait(s_at)
            if s_at < 2:
                yg.send(s_at + 1)
            hand_over(s_at + 1)
            hand_over(7 - s_at)
            if s_at == 1:
                with jax.named_scope("a2a_wait#far"):
                    for slot in slots:
                        if slot > 0:
                            a2a[1, slot].wait_recv()
                hand_over(4)
            if s_at == 0:
                multiply(0, True)
            else:
                multiply(s_at)
                multiply(8 - s_at)
            if s_at == 2:
                multiply(4)
            yield
        multiply(3)
        multiply(5)
        gate, up = acc[mine, 0:HD], acc[mine, HD : 2 * HD]
        hidden = (gate / (1.0 + jnp.exp(-gate)) * up).astype(BF16)
        with jax.named_scope("down"):
            part = dot(hidden, wd[...])
            for p in range(NY):
                lower = part[:, p * 256 : p * 256 + HD]
                upper = part[:, p * 256 + HD : (p + 1) * 256]
                po[p, mine, :] = jnp.where(c == 0, lower, upper)
                tosend[p, mine, :] = jnp.where(c == 0, upper, lower).astype(BF16)
        trade = rdma(
            tosend.at[:, mine, :], fromp.at[:, mine, :], ex_s.at[part_at], ex_r.at[part_at], partner
        )
        trade.start()
        yield
        right = device(z, x, lax.rem(y + 1, NY), c)
        left = device(z, x, lax.rem(y + NY - 1, NY), c)
        moved = []
        last = {}
        half = PART // 2
        for s_at in range(4):
            i_r, i_l = 4 - s_at, 4 + s_at
            if s_at == 0:
                with jax.named_scope("trade_wait"):
                    trade.wait_recv()
            if s_at == 0:
                spans_r, spans_l = ((0, half, False),), ((half, half, False),)
            elif s_at == 1:
                spans_r = ((0, half, True), (half, half, False))
                spans_l = ((0, half, False), (half, half, True))
            else:
                spans_r = spans_l = ((0, PART, True),)
            for way, i, spans, sent, got, to, sems in (
                (0, i_r, spans_r, sbr, rbr, right, (rs_sem[0], rs_sem[1])),
                (1, i_l, spans_l, sbl, rbl, left, (rs_sem[2], rs_sem[3])),
            ):
                if s_at > 0:
                    with jax.named_scope(f"rs_wait#s={s_at}"):
                        last[way].wait_recv()
                p = lax.rem(y + i, NY)
                for at, count, add in spans:
                    rows = pl.ds(base + at, count)
                    value = po[p, rows, :] + fromp[p, rows, :].astype(F32)
                    if add:
                        value = value + got[s_at - 1, rows, :].astype(F32)
                    sent[s_at, rows, :] = value.astype(BF16)
                lo = spans[0][0]
                n = sum(span[1] for span in spans)
                rows = pl.ds(base + lo, n)
                copy = rdma(
                    sent.at[s_at, rows, :], got.at[s_at, rows, :],
                    sems[0].at[part_at, s_at], sems[1].at[part_at, s_at], to,
                )
                copy.start()
                moved.append(copy)
                last[way] = copy
            yield
        with jax.named_scope("rs_wait#s=4"):
            last[0].wait_recv()
            last[1].wait_recv()
        value = po[y, mine, :] + fromp[y, mine, :].astype(F32)
        value = value + rbr[3, mine, :].astype(F32) + rbl[3, mine, :].astype(F32)
        res[mine, :] = value.astype(BF16)
        if part_at == 0:
            ret[pl.ds(0, CAP), :] = value[0:CAP, :].astype(BF16)
        for slot in slots:
            if slot > 0:
                zz, xx = peer(slot, -1)
                at = pl.ds(slot * CAP, CAP)
                back[slot] = rdma(
                    res.at[at, :], ret.at[at, :], back_s.at[slot], back_r.at[slot],
                    device(zz, xx, y, c),
                )
                back[slot].start()
        yield
        for copy in (*across.values(), trade, *moved):
            copy.wait_send()
        yield

    def route_weights():
        l_rw.wait()
        weight = first * rw[0:1, :] + second * rw[1:2, :]
        w_high = weight.astype(BF16)
        w_low = (weight - w_high.astype(F32)).astype(BF16)
        mask = pt[...].astype(F32)
        wth[...] = (dot(spread, w_high) * mask).astype(BF16)
        wtl[...] = (dot(spread, w_low) * mask).astype(BF16)
        yield

    def combine():
        with jax.named_scope("back_wait"):
            for slot in range(1, NEP):
                back[slot].wait_recv()
        over_slots = ((0,), (0,))
        combined = dot(wth[...], ret[...], over_slots) + dot(wtl[...], ret[...], over_slots)
        out_ab[1] = combined.astype(BF16)
        for copy in back.values():
            copy.wait_send()
        yield

    tasks = {str(i): experts(i) for i in range(PARTS)}
    tasks.update({"K": key_side(), "V": value_side(), "O": out_side(), "D": opposite_rows(), "W": route_weights(), "C": combine()})
    for name in ORDER:
        order_done.append(name)
        if name in tasks:
            try:
                with jax.named_scope(name):
                    next(tasks[name])
            except StopIteration:
                del tasks[name]
    for rest in tasks.values():
        with jax.named_scope("rest"):
            for _ in rest:
                pass
    with jax.named_scope("drain"):
        for copy in a2a.values():
            copy.wait_send()
        for ring in drains:
            ring.drain()


def ring_sems(count, steps):
    return [pltpu.SemaphoreType.DMA((count, steps))] * 4


def on_device(
    mixer_input, mixer_gain, query_weight, key_weight, value_weight, score_offset, out_weight,
    expert_input, expert_gain, route_ids, route_weights, gate_weight, up_weight, down_weight,
):
    hbm = pl.BlockSpec(memory_space=pl.ANY)
    vmem = pl.BlockSpec(memory_space=pltpu.VMEM)
    dma = pltpu.SemaphoreType.DMA
    out = pltpu.VMEM((2, ROWS, HD), BF16)
    scratch = [
        pltpu.VMEM((1, 1), F32),
        pltpu.VMEM((ROWS, D), BF16),
        pltpu.VMEM((1, D), F32),
        pltpu.VMEM((D, 3 * HD), BF16),
        pltpu.VMEM((D, HD), BF16),
        pltpu.VMEM((ROWS, D), BF16),
        pltpu.VMEM((1, D), F32),
        pltpu.VMEM((2, ROWS), jnp.int32),
        pltpu.VMEM((2, ROWS), F32),
        pltpu.VMEM((D, 2 * HD), BF16),
        pltpu.VMEM((HD, D), BF16),
        pltpu.VMEM((ROWS, D), BF16),
        pltpu.VMEM((ROWS, HD), BF16),
        pltpu.VMEM((NEP * ROWS, HD), BF16),
        pltpu.VMEM((NEP * ROWS, HD), BF16),
        pltpu.VMEM((ROWS, NEP * ROWS), BF16),
        pltpu.VMEM((ROWS, ROWS), F32),
        pltpu.VMEM((256, 256), BF16),
        pltpu.VMEM((NY, ROWS, 2 * HD), BF16),
        pltpu.VMEM((2, SLOTS, HD), BF16),
        pltpu.VMEM((SLOTS, ROWS), BF16),
        pltpu.VMEM((SLOTS, ROWS), BF16),
        pltpu.VMEM((SLOTS, ROWS), BF16),
        pltpu.VMEM((NY, SLOTS, 2 * HD), BF16),
        pltpu.VMEM((SLOTS, 2 * HD), F32),
        pltpu.VMEM((NY, SLOTS, HD), F32),
        pltpu.VMEM((NY, SLOTS, HD), BF16),
        pltpu.VMEM((NY, SLOTS, HD), BF16),
        pltpu.VMEM((4, SLOTS, HD), BF16),
        pltpu.VMEM((4, SLOTS, HD), BF16),
        pltpu.VMEM((4, SLOTS, HD), BF16),
        pltpu.VMEM((4, SLOTS, HD), BF16),
        pltpu.VMEM((SLOTS, HD), BF16),
        pltpu.VMEM((SLOTS, HD), BF16),
    ]
    semaphores = [
        dma((14,)),
        dma((2, NEP)), dma((2, NEP)), dma((NEP,)), dma((NEP,)),
        dma((NX,)), dma((NX,)), ring_sems(4, 4), dma((8,)), dma((8,)), ring_sems(4, 2),
        dma((8,)), dma((8,)), dma((NY,)), dma((NY,)),
        ring_sems(PARTS, 4), dma((PARTS, NY)), dma((PARTS, NY)),
        dma((PARTS,)), dma((PARTS,)), ring_sems(PARTS, 4),
    ]
    flat, tree = jax.tree.flatten(semaphores)

    def body(*refs):
        def scoped(*sems):
            mega(*refs, *jax.tree.unflatten(tree, sems))

        pl.run_scoped(scoped, *flat)

    both = pl.pallas_call(
        body,
        out_shape=out,
        in_specs=[hbm] * 14,
        out_specs=vmem,
        scratch_shapes=scratch,
        compiler_params=pltpu.CompilerParams(
            collective_id=0, has_side_effects=True, vmem_limit_bytes=60 * 1024 * 1024
        ),
        name="both_halves",
    )(
        score_offset.reshape(1, 1),
        mixer_input, mixer_gain.reshape(1, D), query_weight, key_weight, value_weight, out_weight,
        expert_input, expert_gain.reshape(1, D), route_ids.T, route_weights.T,
        gate_weight.reshape(D, HD), up_weight.reshape(D, HD), down_weight.reshape(HD, D),
    )
    return both[0], both[1]


def solution(mesh):
    in_specs = (
        P("ep", None),
        P(),
        P(None, "tp"),
        P(None, "tp"),
        P(None, "tp"),
        P("tp"),
        P(None, "tp"),
        P("ep", None),
        P(),
        P("ep", None),
        P("ep", None),
        P("ep", None, "tp"),
        P("ep", None, "tp"),
        P("ep", "tp", None),
    )
    out_specs = (P("ep", "tp"), P("ep", "tp"))
    return jax.shard_map(
        on_device, mesh=mesh, in_specs=in_specs, out_specs=out_specs, check_vma=False
    )
```

time: 89.7 us -> 60.6 us (0.68)
  Pallas kernels: 86.2 us -> 58.3 us
  local copies, waits for them, and re-layouts: 2 us -> 0.63 us
    pallas_call x1, Pallas kernels: 86.2 us -> 58.3 us  [on_device(): pl.pallas_call(body, out_shape=out, in_specs=[hbm] * 14, out_specs=vmem,...]
    unnamed x4 -> x0, local copies, waits for them, and re-layouts: 2 us -> none
where the time goes in v2:
time: 60.6 us; the launch traced here: 60.3 us
  Pallas kernels  58.3 us (96%)
  between operations  1.29 us (2%)
  local copies, waits for them, and re-layouts  0.63 us (1%)
    pallas_call x1, Pallas kernels, on_device(): pl.pallas_call(body, out_shape=out, in_specs=[hbm] * 14, out_specs=vmem,...  58.3 us

profile of v2, /device:TPU:1, one launch (start us, length us, event | category | flops | bytes accessed | tf_op | source)
XLA Modules:
  0.0 60.3 jit_solution(14484531318567512615)
XLA Ops:
  1.3 58.3 %both_halves.1 = bf16[2,128,128]{2,1,0:T(8,128)(2,1)S(1)} custom-call(f32[1,1]{1,0:T(1,128)} %bitcast.12.refs_0_, bf16[128,2048]{1,0:T(8,128)(2,1)} %refs_1_.1, f32[1,2048]{1,0:T(1,128)} %bitcast.16, bf16[2048,128]{1,0:T(8,128)(2,1)} %refs_3_.1, bf16[2048,128]{1,0:T(8,128)(2,1)} %refs_4_.1, bf16[2048,128]{1,0:T(8,128)(2,1)} %refs_5_.1, ...), custom_call_target="tpu_custom_call" | custom-call | tf_op jit(solution)/shard_map/both_halves/pallas_call | solution.py:696
  59.6 0.6 %slice_bitcast_fusion = (bf16[128,128]{1,0:T(8,128)(2,1)}, bf16[128,128]{1,0:T(8,128)(2,1)}) fusion(bf16[2,128,128]{2,1,0:T(8,128)(2,1)S(1)} %both_halves.1), kind=kLoop, calls=%fused_computation | loop fusion | bytes 131072 | tf_op jit(solution)/shard_map/squeeze | solution.py:712

commit v3 on v2

--- a/solution.py
+++ b/solution.py
@@ -24,10 +24,10 @@
 PARTS = SLOTS // PART
 ORDER = "".join(
     (
-        "VKD0K12V30123KK01K23K0KV",
-        "1K0213KK0213KK230KV1KK2W",
-        "3V0K1KK2K3K0K1VO23O1023O",
-        "OC",
+        "VWDK012VK301G2K301KV2K3K",
+        "0GK10K23K1K03VK123GKK0VK",
+        "2G1G3KG0KGK2KG1VO032FO13",
+        "2FOOXC",
     )
 )
 
@@ -126,8 +126,8 @@
     out_ab,
     off, xa, ga, wqkv, wo, xb, gb, ids, rw, wgu, wd,
     na, q, kg, vg, wts, cum, suf, att,
-    pk, pt, wth, wtl, xg, acc, po, tosend, fromp, sbr, sbl, rbr, rbl, res, ret,
-    in_sem, a2a_s, a2a_r, back_s, back_r,
+    pk, pt, wth, wtl, xg, acc, po, tosend, fromp, sbr, sbl, rbr, rbl, res, ret, far, farin,
+    in_sem, a2a_s, a2a_r, back_s, back_r, far_s, far_r,
     kx_s, kx_r, kz_sem, vz_s, vz_r, vx_sem, at_s, at_r, atp_s, atp_r,
     yg_sem, ygp_s, ygp_r, ex_s, ex_r, rs_sem,
 ):
@@ -142,6 +142,24 @@
 
     partner = device(z, x, y, other)
     my_cols = pl.ds(pl.multiple_of(c * HD, HD), HD)
+
+    barrier = pltpu.get_barrier_semaphore()
+
+    def peer(slot, sign):
+        dz = DZ_ORDER[slot // NX]
+        dx = slot % NX
+        if sign > 0:
+            return lax.rem(z + dz, NZ), lax.rem(x + dx, NX)
+        return lax.rem(z + (NZ - dz), NZ), lax.rem(x + (NX - dx), NX)
+
+    greet = [partner]
+    greet.append(device(z, x, lax.rem(y + 1, NY), c))
+    greet.append(device(z, x, lax.rem(y + NY - 1, NY), c))
+    for slot in range(NEP - 1, 0, -1):
+        zz, xx = peer(slot, 1)
+        greet.append(device(zz, xx, y, c))
+    for to in greet:
+        pl.semaphore_signal(barrier, inc=1, device_id=to, device_id_type=MESH)
 
     loads = []
 
@@ -162,24 +180,6 @@
     l_wd = load(wd_h, wd)
     l_wo = load(wo_h, wo)
     l_off = load(off_h, off)
-
-    barrier = pltpu.get_barrier_semaphore()
-
-    def peer(slot, sign):
-        dz = DZ_ORDER[slot // NX]
-        dx = slot % NX
-        if sign > 0:
-            return lax.rem(z + dz, NZ), lax.rem(x + dx, NX)
-        return lax.rem(z + (NZ - dz), NZ), lax.rem(x + (NX - dx), NX)
-
-    greet = [partner]
-    greet.append(device(z, x, lax.rem(y + 1, NY), c))
-    greet.append(device(z, x, lax.rem(y + NY - 1, NY), c))
-    for slot in range(NEP - 1, 0, -1):
-        zz, xx = peer(slot, 1)
-        greet.append(device(zz, xx, y, c))
-    for to in greet:
-        pl.semaphore_signal(barrier, inc=1, device_id=to, device_id_type=MESH)
 
     l_ids.wait()
     expert = lax.broadcasted_iota(jnp.int32, (NEP, ROWS), 0)
@@ -246,13 +246,12 @@
     qkv = dot(na[...], wqkv[...])
     q[...] = qkv[:, 0:HD].astype(BF16)
     own_k = pl.ds(pl.multiple_of(ep * ROWS, ROWS), ROWS)
-    own_v = pl.ds(pl.multiple_of((x * NZ + z) * ROWS, ROWS), ROWS)
+    own_v = pl.ds(pl.multiple_of(x * ROWS, ROWS), ROWS)
     kg[own_k, :] = qkv[:, HD : 2 * HD].astype(BF16)
-    vg[own_v, :] = qkv[:, 2 * HD : 3 * HD].astype(BF16)
+    vg[z, own_v, :] = qkv[:, 2 * HD : 3 * HD].astype(BF16)
     suf_j = lax.broadcasted_iota(jnp.int32, (256, 256), 0) & (ROWS - 1)
     suf_s = lax.broadcasted_iota(jnp.int32, (256, 256), 1)
     suf[...] = jnp.where((suf_j > suf_s) | (suf_s >= ROWS), 1.0, 0.0).astype(BF16)
-    cum[...] = jnp.zeros_like(cum)
 
     with jax.named_scope("barrier_wait"):
         pl.semaphore_wait(barrier, len(greet))
@@ -286,19 +285,26 @@
             causal = (k_off + g * 512) < q_pos
             soft = jnp.maximum(zf, 0.0) + jnp.log(1.0 + jnp.exp(-jnp.abs(zf)))
             keep = jnp.where(causal, -soft, 0.0)
-            later = cum[...]
+            later = None
             for b in range(NX - 1, -1, -1):
                 cut = slice(b * ROWS, (b + 1) * ROWS)
                 kb = keep[:, cut]
                 high = kb.astype(BF16)
                 low = (kb - high.astype(F32)).astype(BF16)
                 sums = dot(jnp.concatenate([high, low], axis=1), suf[...])
-                arg = zf[:, cut] + kb + sums[:, :ROWS] + later
+                arg = zf[:, cut] + kb + sums[:, :ROWS]
+                if later is not None:
+                    arg = arg + later
                 w = jnp.where(causal[:, cut], jnp.exp(arg), 0.0).astype(BF16)
-                at = pl.multiple_of((b * NZ + g) * ROWS, ROWS)
-                wts[:, pl.ds(at, ROWS)] = w
-                later = later + sums[:, ROWS:]
-            cum[...] = later
+                wts[d, :, cut] = w
+                later = sums[:, ROWS:] if later is None else later + sums[:, ROWS:]
+            cum[d] = later
+
+    def groups():
+        for d, needed in ((0, 2), (1, 6), (7, 6), (2, 10), (6, 10), (3, 14), (5, 14), (4, 18)):
+            assert order_done.count("K") >= needed
+            group(d)
+            yield
 
     def key_side():
         def k_rows(block, at, count):
@@ -328,38 +334,33 @@
             for j in range(1, NX):
                 kx[j - 1].wait_recv()
                 kz[j].send(0)
-        group(0)
         yield
         for s_at in range(4):
             for r in kz:
                 r.wait(s_at)
                 if s_at < 3:
                     r.send(s_at + 1)
-                if r is kz[-1]:
-                    group(s_at + 1)
                 yield
-        for d in (5, 6, 7):
-            group(d)
-            yield
         for copy in kx:
             copy.wait_send()
         yield
 
     def value_side():
-        def v_rows(block, at, count):
-            return vg.at[pl.ds(pl.multiple_of(block * ROWS + at, 16), count), :]
+        def v_rows(plane, planes, block, at, count):
+            rows = pl.ds(pl.multiple_of(block * ROWS + at, 16), count)
+            return vg.at[pl.ds(plane, planes), rows, :]
 
         vz = TwoStage(
             "vz", z, ROWS,
-            lambda p, at, count: v_rows(x * NZ + p, at, count),
+            lambda p, at, count: v_rows(p, 1, x, at, count),
             lambda p: device(p, x, y, c),
             (vz_s, vz_r),
         )
         vx = [
             Ring(
                 "vx", NX, x,
-                lambda p, i=i: v_rows(p * NZ, i * 256, 256),
-                lambda p, h, i=i: v_rows(p * NZ, i * 256 + h * 128, 128),
+                lambda p, i=i: v_rows(2 * i, 2, p, 0, ROWS),
+                lambda p, h, i=i: v_rows(2 * i + h, 1, p, 0, ROWS),
                 lambda p: device(z, p, y, c),
                 [s.at[i] for s in vx_sem],
             )
@@ -390,8 +391,14 @@
         yield
 
     def out_side():
-        assert order_done.count("K") > 20 and order_done.count("V") > 5
-        attended = dot(wts[...], vg[...]).astype(BF16)
+        assert order_done.count("G") > 7 and order_done.count("V") > 5
+        total, later = None, None
+        for d in range(NZ):
+            g = lax.rem(z + (NZ - d), NZ)
+            part = dot(wts[d], vg[g])
+            total = part if d == 0 else total + jnp.exp(later) * part
+            later = cum[d] if d == 0 else later + cum[d]
+        attended = total.astype(BF16)
         att[y, :, my_cols] = attended
         ring = TwoStage(
             "at", y, ROWS,
@@ -443,6 +450,21 @@
         yield
 
     back = {}
+
+    def give_back(i, slots, value):
+        first = slots[0] * CAP
+        res[i, pl.ds(first, PART), :] = value.astype(BF16)
+        if first == 0:
+            ret[i, pl.ds(0, CAP), :] = value[0:CAP, :].astype(BF16)
+        for slot in slots:
+            if slot > 0:
+                zz, xx = peer(slot, -1)
+                at = pl.ds(slot * CAP, CAP)
+                back[i, slot] = rdma(
+                    res.at[i, at, :], ret.at[i, at, :], back_s.at[i, slot], back_r.at[i, slot],
+                    device(zz, xx, y, c),
+                )
+                back[i, slot].start()
 
     def experts(part_at):
         base = part_at * PART
@@ -527,38 +549,24 @@
         left = device(z, x, lax.rem(y + NY - 1, NY), c)
         moved = []
         last = {}
-        half = PART // 2
-        for s_at in range(4):
-            i_r, i_l = 4 - s_at, 4 + s_at
-            if s_at == 0:
-                with jax.named_scope("trade_wait"):
-                    trade.wait_recv()
-            if s_at == 0:
-                spans_r, spans_l = ((0, half, False),), ((half, half, False),)
-            elif s_at == 1:
-                spans_r = ((0, half, True), (half, half, False))
-                spans_l = ((0, half, False), (half, half, True))
-            else:
-                spans_r = spans_l = ((0, PART, True),)
-            for way, i, spans, sent, got, to, sems in (
-                (0, i_r, spans_r, sbr, rbr, right, (rs_sem[0], rs_sem[1])),
-                (1, i_l, spans_l, sbl, rbl, left, (rs_sem[2], rs_sem[3])),
+        with jax.named_scope("trade_wait"):
+            trade.wait_recv()
+        value = po[opposite, mine, :] + fromp[opposite, mine, :].astype(F32)
+        give_back(1, slots, value)
+        for s_at in range(3):
+            for way, i, sent, got, to, sems in (
+                (0, 3 - s_at, sbr, rbr, right, (rs_sem[0], rs_sem[1])),
+                (1, 5 + s_at, sbl, rbl, left, (rs_sem[2], rs_sem[3])),
             ):
+                p = lax.rem(y + i, NY)
+                value = po[p, mine, :] + fromp[p, mine, :].astype(F32)
                 if s_at > 0:
                     with jax.named_scope(f"rs_wait#s={s_at}"):
                         last[way].wait_recv()
-                p = lax.rem(y + i, NY)
-                for at, count, add in spans:
-                    rows = pl.ds(base + at, count)
-                    value = po[p, rows, :] + fromp[p, rows, :].astype(F32)
-                    if add:
-                        value = value + got[s_at - 1, rows, :].astype(F32)
-                    sent[s_at, rows, :] = value.astype(BF16)
-                lo = spans[0][0]
-                n = sum(span[1] for span in spans)
-                rows = pl.ds(base + lo, n)
+                    value = value + got[s_at - 1, mine, :].astype(F32)
+                sent[s_at, mine, :] = value.astype(BF16)
                 copy = rdma(
-                    sent.at[s_at, rows, :], got.at[s_at, rows, :],
+                    sent.at[s_at, mine, :], got.at[s_at, mine, :],
                     sems[0].at[part_at, s_at], sems[1].at[part_at, s_at], to,
                 )
                 copy.start()
@@ -569,19 +577,8 @@
             last[0].wait_recv()
             last[1].wait_recv()
         value = po[y, mine, :] + fromp[y, mine, :].astype(F32)
-        value = value + rbr[3, mine, :].astype(F32) + rbl[3, mine, :].astype(F32)
-        res[mine, :] = value.astype(BF16)
-        if part_at == 0:
-            ret[pl.ds(0, CAP), :] = value[0:CAP, :].astype(BF16)
-        for slot in slots:
-            if slot > 0:
-                zz, xx = peer(slot, -1)
-                at = pl.ds(slot * CAP, CAP)
-                back[slot] = rdma(
-                    res.at[at, :], ret.at[at, :], back_s.at[slot], back_r.at[slot],
-                    device(zz, xx, y, c),
-                )
-                back[slot].start()
+        value = value + rbr[2, mine, :].astype(F32) + rbl[2, mine, :].astype(F32)
+        give_back(0, slots, value)
         yield
         for copy in (*across.values(), trade, *moved):
             copy.wait_send()
@@ -593,23 +590,59 @@
         w_high = weight.astype(BF16)
         w_low = (weight - w_high.astype(F32)).astype(BF16)
         mask = pt[...].astype(F32)
-        wth[...] = (dot(spread, w_high) * mask).astype(BF16)
-        wtl[...] = (dot(spread, w_low) * mask).astype(BF16)
+        wth[...] = (dot(spread, w_high) * mask).T.astype(BF16)
+        wtl[...] = (dot(spread, w_low) * mask).T.astype(BF16)
+        yield
+
+    def combined(i):
+        with jax.named_scope(f"back_wait#i={i}"):
+            for slot in range(1, NEP):
+                back[i, slot].wait_recv()
+        return dot(wth[...], ret[i]) + dot(wtl[...], ret[i])
+
+    half = ROWS // 2
+    hops = []
+
+    def opposite_part():
+        assert "W" in order_done
+        part = combined(1).astype(BF16)
+        far[0] = part[:half, :]
+        far[1] = part[half:, :]
+        between = [device(z, x, lax.rem(y + a, NY), c) for a in (2, NY - 2)]
+        for i in range(2):
+            hops.append(rdma(far.at[i], far.at[i + 2], far_s.at[i], far_r.at[i], between[i]))
+            hops[i].start()
+        yield
+        for i in range(2):
+            with jax.named_scope("far_wait"):
+                hops[i].wait_recv()
+            hops.append(
+                rdma(far.at[i + 2], farin.at[i], far_s.at[i + 2], far_r.at[i + 2], between[i])
+            )
+            hops[i + 2].start()
         yield
 
     def combine():
-        with jax.named_scope("back_wait"):
-            for slot in range(1, NEP):
-                back[slot].wait_recv()
-        over_slots = ((0,), (0,))
-        combined = dot(wth[...], ret[...], over_slots) + dot(wtl[...], ret[...], over_slots)
-        out_ab[1] = combined.astype(BF16)
-        for copy in back.values():
+        with jax.named_scope("farin_wait"):
+            hops[2].wait_recv()
+            hops[3].wait_recv()
+        sums = combined(0)
+        for i in range(2):
+            rows = slice(i * half, (i + 1) * half)
+            out_ab[1, rows, :] = (sums[rows, :] + farin[i].astype(F32)).astype(BF16)
+        yield
+
+    def drain():
+        for copy in (*a2a.values(), *hops):
             copy.wait_send()
+        for slot in range(1, NEP):
+            back[1, slot].wait_send()
+        for ring in drains:
+            ring.drain()
         yield
 
     tasks = {str(i): experts(i) for i in range(PARTS)}
-    tasks.update({"K": key_side(), "V": value_side(), "O": out_side(), "D": opposite_rows(), "W": route_weights(), "C": combine()})
+    tasks.update({"K": key_side(), "V": value_side(), "O": out_side(), "D": opposite_rows(), "W": route_weights(), "C": combine(), "G": groups(), "F": opposite_part(), "X": drain()})
     for name in ORDER:
         order_done.append(name)
         if name in tasks:
@@ -623,10 +656,8 @@
             for _ in rest:
                 pass
     with jax.named_scope("drain"):
-        for copy in a2a.values():
-            copy.wait_send()
-        for ring in drains:
-            ring.drain()
+        for slot in range(1, NEP):
+            back[0, slot].wait_send()
 
 
 def ring_sems(count, steps):
@@ -656,34 +687,36 @@
         pltpu.VMEM((ROWS, D), BF16),
         pltpu.VMEM((ROWS, HD), BF16),
         pltpu.VMEM((NEP * ROWS, HD), BF16),
-        pltpu.VMEM((NEP * ROWS, HD), BF16),
-        pltpu.VMEM((ROWS, NEP * ROWS), BF16),
-        pltpu.VMEM((ROWS, ROWS), F32),
+        pltpu.VMEM((NZ, NX * ROWS, HD), BF16),
+        pltpu.VMEM((NZ, ROWS, NX * ROWS), BF16),
+        pltpu.VMEM((NZ, ROWS, ROWS), F32),
         pltpu.VMEM((256, 256), BF16),
         pltpu.VMEM((NY, ROWS, 2 * HD), BF16),
         pltpu.VMEM((2, SLOTS, HD), BF16),
         pltpu.VMEM((SLOTS, ROWS), BF16),
-        pltpu.VMEM((SLOTS, ROWS), BF16),
-        pltpu.VMEM((SLOTS, ROWS), BF16),
+        pltpu.VMEM((ROWS, SLOTS), BF16),
+        pltpu.VMEM((ROWS, SLOTS), BF16),
         pltpu.VMEM((NY, SLOTS, 2 * HD), BF16),
         pltpu.VMEM((SLOTS, 2 * HD), F32),
         pltpu.VMEM((NY, SLOTS, HD), F32),
         pltpu.VMEM((NY, SLOTS, HD), BF16),
         pltpu.VMEM((NY, SLOTS, HD), BF16),
-        pltpu.VMEM((4, SLOTS, HD), BF16),
-        pltpu.VMEM((4, SLOTS, HD), BF16),
-        pltpu.VMEM((4, SLOTS, HD), BF16),
-        pltpu.VMEM((4, SLOTS, HD), BF16),
-        pltpu.VMEM((SLOTS, HD), BF16),
-        pltpu.VMEM((SLOTS, HD), BF16),
+        pltpu.VMEM((3, SLOTS, HD), BF16),
+        pltpu.VMEM((3, SLOTS, HD), BF16),
+        pltpu.VMEM((3, SLOTS, HD), BF16),
+        pltpu.VMEM((3, SLOTS, HD), BF16),
+        pltpu.VMEM((2, SLOTS, HD), BF16),
+        pltpu.VMEM((2, SLOTS, HD), BF16),
+        pltpu.VMEM((4, ROWS // 2, HD), BF16),
+        pltpu.VMEM((2, ROWS // 2, HD), BF16),
     ]
     semaphores = [
         dma((14,)),
-        dma((2, NEP)), dma((2, NEP)), dma((NEP,)), dma((NEP,)),
+        dma((2, NEP)), dma((2, NEP)), dma((2, NEP)), dma((2, NEP)), dma((4,)), dma((4,)),
         dma((NX,)), dma((NX,)), ring_sems(4, 4), dma((8,)), dma((8,)), ring_sems(4, 2),
         dma((8,)), dma((8,)), dma((NY,)), dma((NY,)),
-        ring_sems(PARTS, 4), dma((PARTS, NY)), dma((PARTS, NY)),
-        dma((PARTS,)), dma((PARTS,)), ring_sems(PARTS, 4),
+        ring_sems(PARTS, 3), dma((PARTS, NY)), dma((PARTS, NY)),
+        dma((PARTS,)), dma((PARTS,)), ring_sems(PARTS, 3),
     ]
     flat, tree = jax.tree.flatten(semaphores)
 

time: 60.6 us -> 58.4 us (0.964)
  Pallas kernels: 58.3 us -> 56.3 us
    pallas_call x1, Pallas kernels: 58.3 us -> 56.3 us  [on_device(): pl.pallas_call(body, out_shape=out, in_specs=[hbm] * 14, out_specs=vmem,...]
where the time goes in v3:
time: 58.4 us; the launch traced here: 58.3 us
  Pallas kernels  56.3 us (96%)
  between operations  1.29 us (2%)
  local copies, waits for them, and re-layouts  0.63 us (1%)
    pallas_call x1, Pallas kernels, on_device(): pl.pallas_call(body, out_shape=out, in_specs=[hbm] * 14, out_specs=vmem,...  56.3 us

profile of v3, /device:TPU:1, one launch (start us, length us, event | category | flops | bytes accessed | tf_op | source)
XLA Modules:
  0.0 58.3 jit_solution(13261172756857530779)
XLA Ops:
  1.3 56.3 %both_halves.1 = bf16[2,128,128]{2,1,0:T(8,128)(2,1)S(1)} custom-call(f32[1,1]{1,0:T(1,128)} %bitcast.12.refs_0_, bf16[128,2048]{1,0:T(8,128)(2,1)} %refs_1_.1, f32[1,2048]{1,0:T(1,128)} %bitcast.16, bf16[2048,128]{1,0:T(8,128)(2,1)} %refs_3_.1, bf16[2048,128]{1,0:T(8,128)(2,1)} %refs_4_.1, bf16[2048,128]{1,0:T(8,128)(2,1)} %refs_5_.1, ...), custom_call_target="tpu_custom_call" | custom-call | tf_op jit(solution)/shard_map/both_halves/pallas_call | solution.py:729
  57.6 0.6 %slice_bitcast_fusion = (bf16[128,128]{1,0:T(8,128)(2,1)}, bf16[128,128]{1,0:T(8,128)(2,1)}) fusion(bf16[2,128,128]{2,1,0:T(8,128)(2,1)S(1)} %both_halves.1), kind=kLoop, calls=%fused_computation | loop fusion | bytes 131072 | tf_op jit(solution)/shard_map/squeeze | solution.py:745
